TPU v7x, 1024 devices: a whole 4x8x16 slice. The times are simulated.
1024 devices in a mesh: sp: 128 (over z, y), tp: 8 (over x, core).
Axes of the slice: x: 4, y: 8, z: 16, core: 2. Of those that a mesh axis runs over, the one named last changes fastest.
Arguments:
- query: bfloat16 [65536, 1024], P('sp', 'tp'), may hold values from -6 to 6
- key: bfloat16 [65536, 1024], P('sp', 'tp'), may hold values from -6 to 6
- value: bfloat16 [65536, 1024], P('sp', 'tp'), may hold values from -6 to 6
- out_grad: bfloat16 [65536, 1024], P('sp', 'tp'), may hold values from -6 to 6
- query_gain: float32 [64], replicated, may hold values from 0.1 to 1.9
- key_gain: float32 [64], replicated, may hold values from 0.1 to 1.9
- rel_bias: float32 [16, 129], P('tp'), may hold values from -3 to 3
Outputs:
- query_grad: bfloat16 [65536, 1024], P('sp', 'tp')
- key_grad: bfloat16 [65536, 1024], P('sp', 'tp')
- value_grad: bfloat16 [65536, 1024], P('sp', 'tp')
- query_gain_grad: float32 [64], replicated
- key_gain_grad: float32 [64], replicated
- bias_grad: float32 [16, 129], P('tp')
All inputs are finite; a program needn't handle non-finite values.
Results may differ from a plain program's by a relative error of at most 0.0095.
Values may be sent and summed in bfloat16 or wider, within the bound.
A program may use at most 32 MiB of HBM per device.

v0:
```python
import functools

import jax
import jax.numpy as jnp
from jax import lax
from jax.sharding import Mesh
from jax.sharding import PartitionSpec as P

SEG = 64
PREV = 8
CLIP = 128
SP = ("sp_0", "sp_1")
SP_TP = ("sp_0", "sp_1", "tp_0", "tp_1")
TP = ("tp_0", "tp_1")


epsilon = 1e-06


def shifted(block, axis, distance):
    devices = range(lax.axis_size(axis))
    route = [(i - distance, i) for i in devices if i - distance in devices]
    return lax.ppermute(block, axis, route)


def over_axes(shard, axes):
    return functools.reduce(lax.psum, axes, shard)


def normalize(head_rows, gain_vector):
    widened = head_rows.astype(jnp.float32)
    row_scale = lax.rsqrt(jnp.mean(widened * widened, axis=-1, keepdims=True) + epsilon)
    unit_rows = widened * row_scale
    return (unit_rows, row_scale, (unit_rows * gain_vector).astype(jnp.bfloat16))


def norm_backward(grad_hat, unit_rows, row_scale, gain_vector):
    grad_unit = grad_hat * gain_vector
    inner_mean = jnp.mean(grad_unit * unit_rows, axis=-1, keepdims=True)
    return (
        row_scale * (grad_unit - unit_rows * inner_mean),
        jnp.sum(grad_hat * unit_rows, axis=(0, 1)),
    )


def bias_matrix(table_row, block):
    tap_count = table_row.shape[0]
    position = jnp.arange(3 * block - 1, dtype=jnp.int32)
    distance = jnp.clip(2 * block - 1 - position, 0, tap_count - 1)
    selected = distance[:, None] == jnp.arange(tap_count, dtype=jnp.int32)[None, :]
    diagonal = jnp.sum(
        jnp.where(selected, table_row[None, :], jnp.zeros((), table_row.dtype)), axis=1
    )
    diagonal = jnp.concatenate(
        [diagonal[block - 1 :], jnp.zeros((1,), diagonal.dtype), diagonal[: block - 1]]
    )
    flattened = jnp.tile(diagonal, block)[: block * (3 * block - 1)]
    return flattened.reshape(block, 3 * block - 1)[:, : 2 * block]


def tap_totals(score_grad, tap_count):
    block = score_grad.shape[0]
    widened = jnp.pad(score_grad, ((0, 0), (0, block - 1)))
    flattened = jnp.pad(widened.reshape(-1), (0, block))
    columns = jnp.sum(flattened.reshape(block, 3 * block), axis=0)
    near_taps = columns[block - tap_count + 2 : block + 1][::-1]
    return jnp.concatenate([near_taps, (jnp.sum(columns) - jnp.sum(near_taps))[None]])


def band_mask(block):
    row_index = jnp.arange(block, dtype=jnp.int32)[:, None]
    col_index = jnp.arange(2 * block, dtype=jnp.int32)[None, :]
    return (row_index + block >= col_index) & (col_index // SEG >= row_index // SEG)


def block_gradients(
    query_block, key_block, value_block, grad_block, bias_block, allowed, score_scale
):
    scores = (
        jnp.dot(query_block, key_block.T, preferred_element_type=jnp.float32) * score_scale
        + bias_block
    )
    normalizer = jnp.sum(
        jnp.where(allowed, jnp.exp(scores), jnp.zeros((), jnp.float32)), axis=1, keepdims=True
    )
    log_total = jnp.log(normalizer)
    attention = jnp.where(allowed, jnp.exp(scores - log_total), jnp.zeros((), jnp.float32))
    attention_low = attention.astype(jnp.bfloat16)
    output_low = jnp.dot(attention_low, value_block, preferred_element_type=jnp.float32).astype(
        jnp.bfloat16
    )
    output_low = lax.optimization_barrier(output_low)
    row_delta = jnp.sum(
        grad_block.astype(jnp.float32) * output_low.astype(jnp.float32), axis=1, keepdims=True
    )
    attention_grad = jnp.dot(grad_block, value_block.T, preferred_element_type=jnp.float32)
    score_grad = attention * (attention_grad - row_delta)
    score_low = score_grad.astype(jnp.bfloat16)
    query_part = jnp.dot(score_low, key_block, preferred_element_type=jnp.float32) * score_scale
    key_part = jnp.dot(score_low.T, query_block, preferred_element_type=jnp.float32) * score_scale
    value_part = jnp.dot(attention_low.T, grad_block, preferred_element_type=jnp.float32)
    tap_part = tap_totals(score_grad, CLIP + 1)
    return (query_part, key_part, value_part, tap_part, log_total, row_delta)


def per_device(query, key, value, out_grad, query_gain, key_gain, rel_bias):
    block = PREV * SEG
    row_count = query.shape[0]
    local_heads = rel_bias.shape[0]
    head_width = query.shape[1] // local_heads
    score_scale = head_width ** (-0.5)
    shape = (row_count, local_heads, head_width)
    query_unit, query_scale, query_hat = normalize(query.reshape(shape), query_gain)
    key_unit, key_scale, key_hat = normalize(key.reshape(shape), key_gain)
    value_rows = value.reshape(shape)
    grad_rows = out_grad.reshape(shape)
    tail_start = row_count - block
    before_key, before_value = shifted((key_hat, value_rows), SP, 1)
    key_heads = jnp.concatenate([before_key, key_hat]).transpose(1, 0, 2)
    value_heads = jnp.concatenate([before_value, value_rows]).transpose(1, 0, 2)
    query_heads = query_hat.transpose(1, 0, 2)
    grad_heads = grad_rows.transpose(1, 0, 2)
    inside = band_mask(block)
    later = jnp.arange(2 * block, dtype=jnp.int32)[None, :] >= block
    leading = inside & (later | (lax.axis_index(SP) > 0))

    def per_head(items):
        query_part, key_part, value_part, grad_part, table_row = items
        bias_block = bias_matrix(table_row, block)
        key_total = jnp.zeros((row_count + block, head_width), jnp.float32)
        value_total = jnp.zeros((row_count + block, head_width), jnp.float32)
        first_stats = None
        results = block_gradients(
            query_part, key_part, value_part, grad_part, bias_block, leading, score_scale
        )
        query_pieces = [results[0]]
        key_total = key_total.at[0 : 2 * block].add(results[1])
        value_total = value_total.at[0 : 2 * block].add(results[2])
        tap_total = results[3]
        first_stats = (results[4], results[5])
        return (
            jnp.concatenate(query_pieces),
            key_total,
            value_total,
            tap_total,
            first_stats[0],
            first_stats[1],
            bias_block[:, :block],
        )

    query_hat_grad, key_total, value_total, tap_grads, log_totals, row_deltas, bias_blocks = (
        lax.map(per_head, (query_heads, key_heads, value_heads, grad_heads, rel_bias))
    )
    key_own = key_total[:, block:]
    value_own = value_total[:, block:]
    back_key, back_value = (
        shifted(key_total[:, :block].astype(jnp.bfloat16), SP, -1).astype(jnp.float32),
        shifted(value_total[:, :block].astype(jnp.bfloat16), SP, -1).astype(jnp.float32),
    )
    key_own = key_own.at[:, tail_start:].add(back_key)
    value_own = value_own.at[:, tail_start:].add(back_value)
    query_grad, query_gain_part = norm_backward(
        query_hat_grad.transpose(1, 0, 2), query_unit, query_scale, query_gain
    )
    key_grad, key_gain_part = norm_backward(
        key_own.transpose(1, 0, 2), key_unit, key_scale, key_gain
    )
    bias_grad = over_axes(tap_grads, SP)
    query_gain_grad, key_gain_grad = (
        over_axes(query_gain_part, SP_TP),
        over_axes(key_gain_part, SP_TP),
    )
    flat_width = local_heads * head_width
    value_grad = value_own.transpose(1, 0, 2).reshape(row_count, flat_width)
    return (
        query_grad.reshape(row_count, flat_width).astype(jnp.bfloat16),
        key_grad.reshape(row_count, flat_width).astype(jnp.bfloat16),
        value_grad.astype(jnp.bfloat16),
        query_gain_grad,
        key_gain_grad,
        bias_grad,
    )


def solution(mesh):
    torus = Mesh(mesh.devices.reshape(16, 8, 4, 2), ("sp_0", "sp_1", "tp_0", "tp_1"))
    return jax.shard_map(
        per_device,
        mesh=torus,
        in_specs=(P(SP, TP), P(SP, TP), P(SP, TP), P(SP, TP), P(), P(), P(TP, None)),
        out_specs=(P(SP, TP), P(SP, TP), P(SP, TP), P(), P(), P(TP, None)),
        check_vma=False,
    )
```

profile of v0, /device:TPU:1, one launch (start us, length us, event | category | flops | bytes accessed | tf_op | source)
XLA Modules:
  0.0 170.3 jit_solution(7057943459122211764)
XLA Ops:
  0.6 1.0 copy.34
  1.7 4.0 %collective-permute-start.1 = (bf16[512,2,64]{0,2,1:T(8,128)(2,1)S(1)}, bf16[512,2,64]{0,2,1:T(8,128)(2,1)S(1)}, u32[]{:S(2)}, u32[]{:S(2)}) collective-permute-start(bf16[512,2,64]{0,2,1:T(8,128)(2,1)S(1)} %bitcast.132), channel_id=1, source_target_pairs={{0,8},{8,16},{16,24},{24,32},{32,40},{40,48},{48,56},{56,64},{64,7... | collective-permute-start | bytes 393224 | tf_op jit(solution)/shard_map/ppermute | solution.py:23
  5.7 1.0 copy.32
  6.8 0.7 multiply_convert_fusion.2
  7.5 3.2 %collective-permute-start = (bf16[512,2,64]{0,2,1:T(8,128)(2,1)S(1)}, bf16[512,2,64]{0,2,1:T(8,128)(2,1)S(1)}, u32[]{:S(2)}, u32[]{:S(2)}) collective-permute-start(bf16[512,2,64]{0,2,1:T(8,128)(2,1)S(1)} %multiply_convert_fusion.2), channel_id=1, source_target_pairs={{0,8},{8,16},{16,24},{24,32},{32,40},{40,48},{48,56},{56,64},{64,7... | collective-permute-start | bytes 393224 | tf_op jit(solution)/shard_map/ppermute | solution.py:23
  10.8 1.0 copy.31
  11.9 1.4 fusion.36
  16.1 62.6 %while.28 = (s32[]{:T(128)}, f32[2,512,64]{1,2,0:T(8,128)}, f32[2,1024,64]{1,2,0:T(8,128)}, f32[2,1024,64]{1,2,0:T(8,128)}, f32[2,129]{1,0:T(2,128)}, /*index=5*...) while((s32[]{:T(128)}, f32[2,512,64]{1,2,0:T(8,128)}, ...), condition=%wide.region_9.10_spmd.clone, body=%wide.region_2.9_spmd.clone.sunk | while | flops 418188672 | bytes 71477720 | solution.py:152
  17.5 1.9 %tile.22 = f32[786432]{0:T(1024)} reshape(f32[512,1536]{1,0:T(8,128)S(1)} %tile.21) | data formatting | bytes 6291456 | tf_op jit(solution)/shard_map/while/body/eval_jaxpr/tile | solution.py:57
  19.4 4.0 %reshape.313 = f32[512,1535]{1,0:T(8,128)S(1)} reshape(f32[785920]{0:T(1024)} %bitcast.128) | data formatting | bytes 6287360 | tf_op jit(solution)/shard_map/while/body/eval_jaxpr/reshape | solution.py:58
  23.4 2.1 %select_reduce_fusion.5 = (f32[512]{0:T(512)S(1)}, f32[512,1024]{1,0:T(8,128)S(1)}) fusion(pred[1024]{0:T(1024)(128)(4,1)} %get-tuple-element.547, s32[512]{0:T(512)S(1)} %get-tuple-element.545, s32[1024]{0:T(1024)S(1)} %get-tuple-element.546, s32[512]{0:T(512)S(1)} %copy-done.10, f32[512,1535]{1,0:T(8,128)S(1)} %reshape.313, ...), kind=kOutput, calls=%fused_computation.5.clone.1 | convolution fusion | flops 71302656 | bytes 4403200 | tf_op jit(solution)/shard_map/while/body/eval_jaxpr/dot_general | solution.py:80
  25.5 1.3 fusion.72
  27.6 0.8 copy-done.7
  28.5 1.1 subtract_multiply_fusion.2
  30.7 1.0 fusion.74
  31.8 2.1 %pad.51 = f32[512,1535]{1,0:T(8,128)} pad(f32[512,1024]{1,0:T(8,128)S(1)} %subtract_multiply_fusion.2, f32[]{:T(128)} %constant.255.clone.8..sunk), padding=0_0x0_511 | pad | bytes 5240836 | tf_op jit(solution)/shard_map/while/body/eval_jaxpr/jit(_pad)/pad | solution.py:63
  33.8 4.0 %reshape.314 = f32[785920]{0:T(1024)S(1)} reshape(f32[512,1535]{1,0:T(8,128)} %pad.51) | data formatting | bytes 6287360 | tf_op jit(solution)/shard_map/while/body/eval_jaxpr/reshape | solution.py:64
  37.9 3.0 %fusion.76 = (f32[786432]{0:T(1024)}, f32[]{:T(128)}) fusion(f32[785920]{0:T(1024)S(1)} %reshape.314), kind=kLoop, calls=%fused_computation.91.clone.1 | loop fusion | flops 786431 | bytes 6289412 | tf_op jit(solution)/shard_map/while/body/eval_jaxpr/jit(_pad)/pad | solution.py:64
  40.9 2.8 %reshape.315 = f32[512,1536]{1,0:T(8,128)S(1)} reshape(f32[786432]{0:T(1024)} %get-tuple-element.497) | data formatting | bytes 6291456 | tf_op jit(solution)/shard_map/while/body/eval_jaxpr/reshape | solution.py:65
  46.1 1.3 dynamic_update_slice.45
  48.8 1.9 %tile.22 = f32[786432]{0:T(1024)} reshape(f32[512,1536]{1,0:T(8,128)S(1)} %tile.21) | data formatting | bytes 6291456 | tf_op jit(solution)/shard_map/while/body/eval_jaxpr/tile | solution.py:57
  50.7 4.0 %reshape.313 = f32[512,1535]{1,0:T(8,128)S(1)} reshape(f32[785920]{0:T(1024)} %bitcast.128) | data formatting | bytes 6287360 | tf_op jit(solution)/shard_map/while/body/eval_jaxpr/reshape | solution.py:58
  54.7 2.1 %select_reduce_fusion.5 = (f32[512]{0:T(512)S(1)}, f32[512,1024]{1,0:T(8,128)S(1)}) fusion(pred[1024]{0:T(1024)(128)(4,1)} %get-tuple-element.547, s32[512]{0:T(512)S(1)} %get-tuple-element.545, s32[1024]{0:T(1024)S(1)} %get-tuple-element.546, s32[512]{0:T(512)S(1)} %copy-done.10, f32[512,1535]{1,0:T(8,128)S(1)} %reshape.313, ...), kind=kOutput, calls=%fused_computation.5.clone.1 | convolution fusion | flops 71302656 | bytes 4403200 | tf_op jit(solution)/shard_map/while/body/eval_jaxpr/dot_general | solution.py:80
  56.8 1.3 fusion.72
  58.9 0.8 copy-done.7
  59.8 1.1 subtract_multiply_fusion.2
  62.1 1.0 fusion.74
  63.1 2.1 %pad.51 = f32[512,1535]{1,0:T(8,128)} pad(f32[512,1024]{1,0:T(8,128)S(1)} %subtract_multiply_fusion.2, f32[]{:T(128)} %constant.255.clone.8..sunk), padding=0_0x0_511 | pad | bytes 5240836 | tf_op jit(solution)/shard_map/while/body/eval_jaxpr/jit(_pad)/pad | solution.py:63
  65.1 4.0 %reshape.314 = f32[785920]{0:T(1024)S(1)} reshape(f32[512,1535]{1,0:T(8,128)} %pad.51) | data formatting | bytes 6287360 | tf_op jit(solution)/shard_map/while/body/eval_jaxpr/reshape | solution.py:64
  69.2 3.0 %fusion.76 = (f32[786432]{0:T(1024)}, f32[]{:T(128)}) fusion(f32[785920]{0:T(1024)S(1)} %reshape.314), kind=kLoop, calls=%fused_computation.91.clone.1 | loop fusion | flops 786431 | bytes 6289412 | tf_op jit(solution)/shard_map/while/body/eval_jaxpr/jit(_pad)/pad | solution.py:64
  72.2 2.8 %reshape.315 = f32[512,1536]{1,0:T(8,128)S(1)} reshape(f32[786432]{0:T(1024)} %get-tuple-element.497) | data formatting | bytes 6291456 | tf_op jit(solution)/shard_map/while/body/eval_jaxpr/reshape | solution.py:65
  77.4 1.3 dynamic_update_slice.45
  78.7 1.4 fusion.35
  80.1 1.0 slice.143
  81.1 1.3 collective-permute-start.2
  82.4 1.2 multiply_convert_fusion.1
  83.5 0.8 copy.38
  84.3 1.0 slice.142
  85.3 1.3 collective-permute-start.3
  86.8 1.2 fusion.34
  88.0 1.1 multiply_convert_fusion
  89.0 0.8 copy.39
  89.8 1.8 %collective-permute-done.3 = bf16[2,512,64]{1,2,0:T(8,128)(2,1)S(1)} collective-permute-done((bf16[2,512,64]{1,2,0:T(8,128)(2,1)S(1)}, bf16[2,512,64]{1,2,0:T(8,128)(2,1)S(1)}, u32[]{:S(2)}, u32[]{:S(2)}) %collective-permute-start.3) | collective-permute-done | bytes 131104 | tf_op jit(solution)/shard_map/ppermute | solution.py:23
  91.7 0.8 copy.40
  92.4 38.4 %all-reduce.2 = (f32[64]{0:T(128)S(1)}, f32[64]{0:T(128)S(1)}, f32[2,129]{1,0:T(2,128)S(1)}) all-reduce(f32[64]{0:T(128)S(1)} %get-tuple-element.359, f32[64]{0:T(128)S(1)} %get-tuple-element.357, f32[2,129]{1,0:T(2,128)S(1)} %copy-done.16), channel_id=1, replica_groups=mesh['sp_0'=16,'sp_1'=8,'tp_0'=4,'tp_1'=2] {'sp_0'}, use_global_device_ids=true, to_apply=%region_13.14 | all-reduce | flops 386 | bytes 3088 | tf_op jit(solution)/shard_map/psum | solution.py:27
  130.8 13.0 %all-reduce.3 = (f32[64]{0:T(128)S(1)}, f32[64]{0:T(128)S(1)}, f32[2,129]{1,0:T(2,128)}) all-reduce(f32[64]{0:T(128)S(1)} %get-tuple-element.389, f32[64]{0:T(128)S(1)} %get-tuple-element.390, f32[2,129]{1,0:T(2,128)S(1)} %get-tuple-element.391), channel_id=1, replica_groups=mesh['sp_0'=16,'sp_1'=8,'tp_0'=4,'tp_1'=2] {'sp_1'}, use_global_device_ids=true, to_apply=%region_14.15 | all-reduce | flops 386 | bytes 3088 | tf_op jit(solution)/shard_map/psum | solution.py:27
  143.8 8.4 %all-reduce.4 = (f32[64]{0:T(128)S(1)}, f32[64]{0:T(128)S(1)}) all-reduce(f32[64]{0:T(128)S(1)} %get-tuple-element.392, f32[64]{0:T(128)S(1)} %get-tuple-element.393), channel_id=1, replica_groups=mesh['sp_0'=16,'sp_1'=8,'tp_0'=4,'tp_1'=2] {'tp_0'}, use_global_device_ids=true, to_apply=%region_15.16 | all-reduce | flops 128 | bytes 1024 | tf_op jit(solution)/shard_map/psum | solution.py:27
  152.3 18.0 %all-reduce.5 = (f32[64]{0:T(128)}, f32[64]{0:T(128)}) all-reduce(f32[64]{0:T(128)S(1)} %get-tuple-element.395, f32[64]{0:T(128)S(1)} %get-tuple-element.396), channel_id=1, replica_groups=mesh['sp_0'=16,'sp_1'=8,'tp_0'=4,'tp_1'=2] {'tp_1'}, use_global_device_ids=true, to_apply=%region_16.17 | all-reduce | flops 128 | bytes 1024 | tf_op jit(solution)/shard_map/psum | solution.py:27
  (104 shorter events, 12.1 us)
Async XLA Ops:
  0.6 13.8 %copy-start.9 = (bf16[512,128]{1,0:T(8,128)(2,1)S(1)}, bf16[512,128]{1,0:T(8,128)(2,1)}, u32[]{:S(2)}) copy-start(bf16[512,128]{1,0:T(8,128)(2,1)} %param.28) | copy-start | bytes 393220
  1.7 12.9 %collective-permute-start.1 = (bf16[512,2,64]{0,2,1:T(8,128)(2,1)S(1)}, bf16[512,2,64]{0,2,1:T(8,128)(2,1)S(1)}, u32[]{:S(2)}, u32[]{:S(2)}) collective-permute-start(bf16[512,2,64]{0,2,1:T(8,128)(2,1)S(1)} %bitcast.132), channel_id=1, source_target_pairs={{0,8},{8,16},{16,24},{24,32},{32,40},{40,48},{48,56},{56,64},{64,7... | collective-permute-start | bytes 393224 | tf_op jit(solution)/shard_map/ppermute | solution.py:23
  6.8 4.0 %copy-start.11 = (f32[512,2]{0,1:T(2,128)}, f32[512,2]{0,1:T(2,128)S(1)}, u32[]{:S(2)}) copy-start(f32[512,2]{0,1:T(2,128)S(1)} %add_rsqrt_fusion) | copy-start | bytes 12292
  7.5 7.8 %collective-permute-start = (bf16[512,2,64]{0,2,1:T(8,128)(2,1)S(1)}, bf16[512,2,64]{0,2,1:T(8,128)(2,1)S(1)}, u32[]{:S(2)}, u32[]{:S(2)}) collective-permute-start(bf16[512,2,64]{0,2,1:T(8,128)(2,1)S(1)} %multiply_convert_fusion.2), channel_id=1, source_target_pairs={{0,8},{8,16},{16,24},{24,32},{32,40},{40,48},{48,56},{56,64},{64,7... | collective-permute-start | bytes 393224 | tf_op jit(solution)/shard_map/ppermute | solution.py:23
  11.8 4.3 %copy-start = (f32[512,128]{0,1:T(8,128)}, f32[512,128]{0,1:T(8,128)S(1)}, u32[]{:S(2)}) copy-start(f32[512,128]{0,1:T(8,128)S(1)} %copy.31) | copy-start | bytes 786436
  11.9 4.2 %copy-start.13 = (f32[512,2]{0,1:T(2,128)}, f32[512,2]{0,1:T(2,128)S(1)}, u32[]{:S(2)}) copy-start(f32[512,2]{0,1:T(2,128)S(1)} %add_rsqrt_fusion.1) | copy-start | bytes 12292
  19.4 4.0 %copy-start.10 = (s32[512]{0:T(512)S(1)}, s32[512]{0:T(512)}, u32[]{:S(2)}) copy-start(s32[512]{0:T(512)} %get-tuple-element.544) | copy-start | bytes 6148 | tf_op jit(solution)/shard_map/while
  23.4 2.1 %copy-start.14 = (pred[1024]{0:T(1024)(128)(4,1)S(1)}, pred[1024]{0:T(1024)(128)(4,1)}, u32[]{:S(2)}) copy-start(pred[1024]{0:T(1024)(128)(4,1)} %get-tuple-element.547) | copy-start | bytes 3076 | tf_op jit(solution)/shard_map/while
  25.5 1.3 copy-start.1
  25.5 1.8 %copy-start.6 = (f32[2,1024,64]{1,2,0:T(8,128)S(1)}, f32[2,1024,64]{1,2,0:T(8,128)}, u32[]{:S(2)}) copy-start(f32[2,1024,64]{1,2,0:T(8,128)} %get-tuple-element.519) | copy-start | bytes 1572868 | tf_op jit(solution)/shard_map/while
  27.6 0.8 copy-start.7
  28.4 1.1 copy-start.2
  28.5 1.1 copy-start.4
  29.5 1.2 copy-start.3
  30.0 0.7 copy-start.5
  50.7 4.0 %copy-start.10 = (s32[512]{0:T(512)S(1)}, s32[512]{0:T(512)}, u32[]{:S(2)}) copy-start(s32[512]{0:T(512)} %get-tuple-element.544) | copy-start | bytes 6148 | tf_op jit(solution)/shard_map/while
  54.7 2.1 %copy-start.14 = (pred[1024]{0:T(1024)(128)(4,1)S(1)}, pred[1024]{0:T(1024)(128)(4,1)}, u32[]{:S(2)}) copy-start(pred[1024]{0:T(1024)(128)(4,1)} %get-tuple-element.547) | copy-start | bytes 3076 | tf_op jit(solution)/shard_map/while
  56.8 1.3 copy-start.1
  56.8 1.8 %copy-start.6 = (f32[2,1024,64]{1,2,0:T(8,128)S(1)}, f32[2,1024,64]{1,2,0:T(8,128)}, u32[]{:S(2)}) copy-start(f32[2,1024,64]{1,2,0:T(8,128)} %get-tuple-element.519) | copy-start | bytes 1572868 | tf_op jit(solution)/shard_map/while
  58.9 0.8 copy-start.7
  59.8 1.1 copy-start.2
  59.8 1.1 copy-start.4
  60.9 1.2 copy-start.3
  61.3 0.7 copy-start.5
  78.7 8.1 %copy-start.12 = (f32[512,2]{0,1:T(2,128)S(1)}, f32[512,2]{0,1:T(2,128)}, u32[]{:S(2)}) copy-start(f32[512,2]{0,1:T(2,128)} %copy-done.11) | copy-start | bytes 12292
  78.7 8.1 %copy-start.15 = (f32[64]{0:T(128)S(1)}, f32[64]{0:T(128)}, u32[]{:S(2)}) copy-start(f32[64]{0:T(128)} %param.30) | copy-start | bytes 772
  78.7 12.9 %copy-start.8 = (f32[2,1024,64]{1,2,0:T(8,128)S(1)}, f32[2,1024,64]{1,2,0:T(8,128)}, u32[]{:S(2)}) copy-start(f32[2,1024,64]{1,2,0:T(8,128)} %get-tuple-element.267) | copy-start | bytes 1572868
  80.1 12.3 %copy-start.16 = (f32[2,129]{1,0:T(2,128)S(1)}, f32[2,129]{1,0:T(2,128)}, u32[]{:S(2)}) copy-start(f32[2,129]{1,0:T(2,128)} %get-tuple-element.268) | copy-start | bytes 3100
  81.1 5.7 %collective-permute-start.2 = (bf16[2,512,64]{1,2,0:T(8,128)(2,1)S(1)}, bf16[2,512,64]{1,2,0:T(8,128)(2,1)S(1)}, u32[]{:S(2)}, u32[]{:S(2)}) collective-permute-start(bf16[2,512,64]{1,2,0:T(8,128)(2,1)S(1)} %slice.143), channel_id=1, source_target_pairs={{8,0},{16,8},{24,16},{32,24},{40,32},{48,40},{56,48},{64,56},{72,6... | collective-permute-start | bytes 393224 | tf_op jit(solution)/shard_map/ppermute | solution.py:23
  85.3 6.3 %collective-permute-start.3 = (bf16[2,512,64]{1,2,0:T(8,128)(2,1)S(1)}, bf16[2,512,64]{1,2,0:T(8,128)(2,1)S(1)}, u32[]{:S(2)}, u32[]{:S(2)}) collective-permute-start(bf16[2,512,64]{1,2,0:T(8,128)(2,1)S(1)} %slice.142), channel_id=1, source_target_pairs={{8,0},{16,8},{24,16},{32,24},{40,32},{48,40},{56,48},{64,56},{72,6... | collective-permute-start | bytes 393224 | tf_op jit(solution)/shard_map/ppermute | solution.py:23
where the time goes:
time: 171 us; the launch traced here: 170 us
  blocking collectives  77.8 us (45%)
  local copies, waits for them, and re-layouts  45.4 us (27%)
  other arithmetic  20.6 us (12%)
  matrix products  10.7 us (6%)
  starting transfers between devices  9.81 us (6%)
  loops' own time  3.06 us (2%)
  waiting for transfers between devices  2.05 us (1%)
    psum x4, blocking collectives, over_axes(): return functools.reduce(lax.psum, axes, shard)  77.8 us
    ppermute x4, starting transfers between devices, shifted(): return lax.ppermute(block, axis, route)  9.81 us
    reshape x2, local copies, waits for them, and re-layouts, tap_totals(): flattened = jnp.pad(widened.reshape(-1), (0, block))  8.1 us
    reshape x2, local copies, waits for them, and re-layouts, bias_matrix(): return flattened.reshape(block, 3 * block - 1)[:, :2 * block]  7.97 us
    pad x2, other arithmetic, tap_totals(): flattened = jnp.pad(widened.reshape(-1), (0, block))  6.01 us
    reshape x2, local copies, waits for them, and re-layouts, tap_totals(): columns = jnp.sum(flattened.reshape(block, 3 * block), axis=0)  5.63 us
    another operation x4, local copies, waits for them, and re-layouts, bias_matrix(): flattened = jnp.tile(diagonal, block)[:block * (3 * block - 1)]  4.49 us
    dot_general x2, matrix products, block_gradients(): jnp.dot(query_block, key_block.T, preferred_element_type=jnp.float32)  4.14 us
  transfers between devices with their start and end apart: 4, of which 2 were waited for; matrix products, arithmetic and copies ran while one was open for 7% of the time, Pallas kernels for 0%

commit v1 on v0

v1 whole, which is shorter than its diff:
```python
import functools

import jax
import jax.numpy as jnp
from jax import lax
from jax.experimental import pallas as pl
from jax.experimental.pallas import tpu as pltpu
from jax.sharding import Mesh
from jax.sharding import PartitionSpec as P

SP = ("z", "y")
TP = ("x", "c")
MESH = pl.DeviceIdType.MESH

ROWS = 512
TILE = 128
TILES = ROWS // TILE
LANES = 128
HD = 64
WIDE = 2 * TILE
EPS = 1e-06
LOG2E = 1.4426950408889634
SCALE = HD**-0.5
OFF = -1e30

f32 = jnp.float32
bf16 = jnp.bfloat16


def dot(a, b, dims=((1,), (0,))):
    return lax.dot_general(a, b, (dims, ((), ())), preferred_element_type=f32)


def iota(shape, axis):
    return lax.broadcasted_iota(jnp.int32, shape, axis)


def head_sums(x, ones):
    high = x.astype(bf16)
    low = (x - high.astype(f32)).astype(bf16)
    return dot(high, ones) + dot(low, ones)


def normalize(x, gain, ones):
    wide = x.astype(f32)
    scale = lax.rsqrt(head_sums(wide * wide, ones) * (1.0 / HD) + EPS)
    unit = wide * scale
    return unit, scale, (unit * gain).astype(bf16)


def norm_backward(grad_hat, unit, scale, gain, ones):
    grad_unit = grad_hat * gain
    inner = head_sums(grad_unit * unit, ones) * (1.0 / HD)
    return scale * (grad_unit - unit * inner)


def shifted_rows(row):
    rows = jnp.broadcast_to(row, (8, LANES))
    index = iota((8, LANES), 0)
    for bit in (1, 2, 4):
        rows = jnp.where((index & bit) != 0, pltpu.roll(rows, bit, 1), rows)
    size = 8
    while size < TILE:
        rows = jnp.concatenate([rows, pltpu.roll(rows, size, 1)], axis=0)
        size *= 2
    return rows


def diagonal_sums(block):
    size = TILE
    while size > 8:
        size //= 2
        block = block[:size] + pltpu.roll(block[size:], LANES - size, 1)
    index = iota((8, LANES), 0)
    for bit in (1, 2, 4):
        block = jnp.where((index & bit) != 0, pltpu.roll(block, LANES - bit, 1), block)
    return jnp.sum(block, axis=0, keepdims=True)


def both_heads(a):
    first = iota((TILE, LANES), 1) < HD
    zero = jnp.zeros((), a.dtype)
    return jnp.concatenate([jnp.where(first, a, zero), jnp.where(first, zero, a)], axis=0)


def body(
    sizes,
    q_ref,
    k_ref,
    v_ref,
    g_ref,
    qgain_ref,
    kgain_ref,
    bias_ref,
    dq_ref,
    dk_ref,
    dv_ref,
    dqgain_ref,
    dkgain_ref,
    dbias_ref,
    hk_ref,
    hv_ref,
    nq_ref,
    ng_ref,
    send_stat,
    recv_stat,
    unit_q,
    scale_q,
    khat_ref,
    hkhat_ref,
    qm_ref,
    gm_ref,
    qmn_ref,
    gmn_ref,
    e_ref,
    d_ref,
    en_ref,
    dn_ref,
    pown_ref,
    sown_ref,
    pn_ref,
    sn_ref,
    ybuf,
    zbuf,
    tbuf,
    halo_send,
    halo_recv,
    stat_ssem,
    stat_rsem,
    y_ssem,
    y_rsem,
    z_ssem,
    z_rsem,
    t_ssem,
    t_rsem,
):
    nz, ny, nx, nc = sizes
    nsp, ntp = nz * ny, nx * nc
    z, y, x, c = (lax.axis_index(a) for a in ("z", "y", "x", "c"))
    sp = z * ny + y
    after, before = lax.rem(sp + 1, nsp), lax.rem(sp + nsp - 1, nsp)
    t_me = x * nc + c

    def at_sp(i):
        return {"z": i // ny, "y": lax.rem(i, ny)}

    def at_tp(i):
        return {"x": i // nc, "c": lax.rem(i, nc)}

    y_peers = [lax.rem(y + d, ny) for d in range(1, ny)]
    z_peers = [lax.rem(z + d, nz) for d in range(1, nz)]
    t_peers = [lax.rem(t_me + d, ntp) for d in range(1, ntp)]

    barrier = pltpu.get_barrier_semaphore()
    targets = [at_sp(after), at_sp(before)]
    targets += [{"y": p} for p in y_peers]
    targets += [{"z": p} for p in z_peers]
    targets += [at_tp(p) for p in t_peers]
    for target in targets:
        pl.semaphore_signal(barrier, inc=1, device_id=target, device_id_type=MESH)
    pl.semaphore_wait(barrier, len(targets))

    def halo_copy(kind, tile):
        src, dst, to = (
            (k_ref, hk_ref, after),
            (v_ref, hv_ref, after),
            (q_ref, nq_ref, before),
            (g_ref, ng_ref, before),
        )[kind]
        rows = pl.ds(tile * TILE, TILE)
        return pltpu.make_async_remote_copy(
            src_ref=src.at[rows],
            dst_ref=dst.at[rows],
            send_sem=halo_send.at[kind, tile],
            recv_sem=halo_recv.at[kind, tile],
            device_id=at_sp(to),
            device_id_type=MESH,
        )

    for tile in reversed(range(TILES)):
        for kind in range(4):
            halo_copy(kind, tile).start()

    ones = (iota((LANES, LANES), 0) // HD == iota((LANES, LANES), 1) // HD).astype(bf16)
    qgain = jnp.concatenate([qgain_ref[...], qgain_ref[...]], axis=1)
    kgain = jnp.concatenate([kgain_ref[...], kgain_ref[...]], axis=1)

    key_i, query_i = iota((TILE, TILE), 0), iota((TILE, TILE), 1)
    reached = query_i >= key_i
    near, mid, far = [], [], []
    for h in range(2):
        row = bias_ref[h : h + 1, 0:LANES] * LOG2E
        last = bias_ref[h : h + 1, LANES : LANES + 1] * LOG2E
        table = shifted_rows(row)
        near.append(jnp.where(reached, table, OFF))
        mid.append(jnp.where(reached, last, table))
        far.append(jnp.broadcast_to(last, (1, TILE)))
    near = jnp.concatenate(near, axis=1)
    mid = jnp.concatenate(mid, axis=1)
    far = jnp.concatenate(far, axis=1)
    both_reached = jnp.concatenate([reached, reached], axis=1)
    wide_q = lax.rem(iota((TILE, WIDE), 1), TILE) // HD
    wide_k = iota((TILE, WIDE), 0) // HD
    edge = jnp.where(wide_k >= wide_q, 0.0, OFF)
    halo_off = jnp.where(sp > 0, 0.0, OFF)
    next_off = jnp.where(sp < nsp - 1, 0.0, OFF)

    def own_bias(distance):
        return (near, mid, far)[min(distance, 2)]

    def halo_bias(distance, off):
        if distance == 0:
            return far + edge + off
        return (mid if distance == TILES - 1 else far) + off

    for t in range(TILES):
        rows = slice(t * TILE, (t + 1) * TILE)
        unit, scale, hat = normalize(q_ref[rows], qgain, ones)
        unit_q[rows] = unit
        scale_q[rows] = scale
        qm_ref[t * WIDE : (t + 1) * WIDE] = both_heads(hat)
        gm_ref[t * WIDE : (t + 1) * WIDE] = both_heads(g_ref[rows])
    khat_ref[...] = normalize(k_ref[...], kgain, ones)[2]

    nt = ((1,), (1,))
    l_parts, n_parts = [], []
    for t in range(TILES):
        cols = slice(t * WIDE, (t + 1) * WIDE)
        count = (t + 1) * TILE
        s = dot(khat_ref[0:count], qm_ref[cols], nt)
        d = dot(v_ref[0:count], gm_ref[cols], nt)
        l_sum = jnp.zeros((1, WIDE), f32)
        n_sum = jnp.zeros((1, WIDE), f32)
        for ck in range(t + 1):
            part = slice(ck * TILE, (ck + 1) * TILE)
            slot = slice((TILES - t + ck) * TILE, (TILES - t + ck + 1) * TILE)
            e = jnp.exp2(s[part] * (SCALE * LOG2E) + own_bias(t - ck))
            e_ref[t, slot] = e
            d_ref[t, slot] = d[part]
            l_sum += jnp.sum(e, axis=0, keepdims=True)
            n_sum += jnp.sum(e * d[part], axis=0, keepdims=True)
        l_parts.append(l_sum)
        n_parts.append(n_sum)

    def stat_copy(t):
        return pltpu.make_async_remote_copy(
            src_ref=send_stat.at[t],
            dst_ref=recv_stat.at[t],
            send_sem=stat_ssem.at[t],
            recv_sem=stat_rsem.at[t],
            device_id=at_sp(before),
            device_id_type=MESH,
        )

    total = jnp.zeros((1, WIDE), f32)
    near_sum = jnp.zeros((TILE, WIDE), f32)
    mid_sum = jnp.zeros((TILE, WIDE), f32)
    gain_sum = jnp.zeros((1, LANES), f32)
    for ck in reversed(range(TILES)):
        rows = slice(ck * TILE, (ck + 1) * TILE)
        halo_copy(0, ck).wait_recv()
        hkhat_ref[rows] = normalize(hk_ref[rows], kgain, ones)[2]
        halo_copy(1, ck).wait_recv()
        span = (ck + 1) * WIDE
        s = dot(hkhat_ref[rows], qm_ref[0:span], nt)
        d = dot(hv_ref[rows], gm_ref[0:span], nt)
        for t in range(ck + 1):
            part = slice(t * WIDE, (t + 1) * WIDE)
            slot = slice((ck - t) * TILE, (ck - t + 1) * TILE)
            e = jnp.exp2(s[:, part] * (SCALE * LOG2E) + halo_bias(ck - t, halo_off))
            e_ref[t, slot] = e
            d_ref[t, slot] = d[:, part]
            l_parts[t] += jnp.sum(e, axis=0, keepdims=True)
            n_parts[t] += jnp.sum(e * d[:, part], axis=0, keepdims=True)
        t = ck
        inv = 1.0 / l_parts[t]
        delta = n_parts[t] * inv
        send_stat[t, 0:1] = inv
        send_stat[t, 1:2] = delta
        stat_copy(t).start()
        cols = slice(t * WIDE, (t + 1) * WIDE)
        prob = e_ref[t] * inv
        grad = prob * (d_ref[t] - delta)
        total += jnp.sum(grad, axis=0, keepdims=True)
        own = (TILES - t) * TILE
        near_sum += grad[TILES * TILE :]
        if t > 0:
            mid_sum += grad[(TILES - 1) * TILE : TILES * TILE]
        else:
            mid_sum += grad[(TILES - 1) * TILE : TILES * TILE]
        low = grad.astype(bf16)
        pown_ref[0 : (t + 1) * TILE, cols] = prob[own:].astype(bf16)
        sown_ref[0 : (t + 1) * TILE, cols] = low[own:]
        keys = jnp.concatenate([hkhat_ref[t * TILE :], khat_ref[0 : (t + 1) * TILE]], axis=0)
        dq_t = dot(keys, low, ((0,), (0,)))
        dq_t = jnp.concatenate([dq_t[0:HD, 0:TILE], dq_t[HD:, TILE:]], axis=0) * SCALE
        grad_hat = dq_t.T
        unit = unit_q[rows]
        gain_sum += jnp.sum(grad_hat * unit, axis=0, keepdims=True)
        dq_ref[rows] = norm_backward(grad_hat, unit, scale_q[rows], qgain, ones).astype(bf16)

    diagonals = jnp.where(both_reached, near_sum, mid_sum)
    taps = [diagonal_sums(diagonals[:, h * TILE : (h + 1) * TILE]) for h in range(2)]
    sums = [jnp.sum(total[:, h * TILE : (h + 1) * TILE], axis=1, keepdims=True) for h in range(2)]
    lane = iota((1, LANES), 1)
    sums = jnp.where(lane < HD, sums[0], sums[1])
    ybuf[y] = jnp.concatenate([taps[0], taps[1], gain_sum, sums], axis=0)

    def y_copy(peer, slot):
        return pltpu.make_async_remote_copy(
            src_ref=ybuf.at[slot],
            dst_ref=ybuf.at[slot],
            send_sem=y_ssem.at[peer],
            recv_sem=y_rsem.at[slot],
            device_id={"y": peer},
            device_id_type=MESH,
        )

    def z_copy(peer, slot):
        return pltpu.make_async_remote_copy(
            src_ref=zbuf.at[slot],
            dst_ref=zbuf.at[slot],
            send_sem=z_ssem.at[peer],
            recv_sem=z_rsem.at[slot],
            device_id={"z": peer},
            device_id_type=MESH,
        )

    def t_copy(peer, slot):
        return pltpu.make_async_remote_copy(
            src_ref=tbuf.at[slot],
            dst_ref=tbuf.at[slot],
            send_sem=t_ssem.at[peer],
            recv_sem=t_rsem.at[slot],
            device_id=at_tp(peer),
            device_id_type=MESH,
        )

    for p in y_peers:
        y_copy(p, y).start()

    for t in reversed(range(TILES)):
        rows = slice(t * TILE, (t + 1) * TILE)
        cols = slice(t * WIDE, (t + 1) * WIDE)
        halo_copy(2, t).wait_recv()
        qmn_ref[cols] = both_heads(normalize(nq_ref[rows], qgain, ones)[2])
        halo_copy(3, t).wait_recv()
        gmn_ref[cols] = both_heads(ng_ref[rows])
        s = dot(khat_ref[t * TILE :], qmn_ref[cols], nt)
        d = dot(v_ref[t * TILE :], gmn_ref[cols], nt)
        for ck in range(t, TILES):
            part = slice((ck - t) * TILE, (ck - t + 1) * TILE)
            rows = slice(ck * TILE, (ck + 1) * TILE)
            en_ref[rows, cols] = jnp.exp2(
                s[part] * (SCALE * LOG2E) + halo_bias(ck - t, next_off)
            )
            dn_ref[rows, cols] = d[part]

    for p in y_peers:
        y_copy(p, p).wait_recv()
    summed = ybuf[0]
    for i in range(1, ny):
        summed += ybuf[i]
    zbuf[z] = summed
    for p in z_peers:
        z_copy(p, z).start()

    for t in reversed(range(TILES)):
        cols = slice(t * WIDE, (t + 1) * WIDE)
        stat_copy(t).wait_recv()
        inv, delta = recv_stat[t, 0:1], recv_stat[t, 1:2]
        prob = en_ref[t * TILE :, cols] * inv
        pn_ref[t * TILE :, cols] = prob.astype(bf16)
        sn_ref[t * TILE :, cols] = (prob * (dn_ref[t * TILE :, cols] - delta)).astype(bf16)

    unit_k, scale_k, _ = normalize(k_ref[...], kgain, ones)
    for ck in range(TILES):
        rows = slice(ck * TILE, (ck + 1) * TILE)
        own, later = slice(ck * WIDE, TILES * WIDE), slice(0, (ck + 1) * WIDE)
        dv = dot(pown_ref[rows, own], gm_ref[own]) + dot(pn_ref[rows, later], gmn_ref[later])
        dv_ref[rows] = dv.astype(bf16)
        dk = dot(sown_ref[rows, own], qm_ref[own]) + dot(sn_ref[rows, later], qmn_ref[later])
        dk_ref[rows] = norm_backward(
            dk * SCALE, unit_k[rows], scale_k[rows], kgain, ones
        ).astype(bf16)

    for p in z_peers:
        z_copy(p, p).wait_recv()
    summed = zbuf[0]
    for i in range(1, nz):
        summed += zbuf[i]
    tbuf[t_me] = summed[2:3]
    for p in t_peers:
        t_copy(p, t_me).start()
    rest = [summed[3:4, h * HD : h * HD + 1] for h in range(2)]
    for h in range(2):
        taps = summed[h : h + 1]
        dbias_ref[h : h + 1, 0:LANES] = taps
        dbias_ref[h : h + 1, LANES : LANES + 1] = rest[h] - jnp.sum(taps, axis=1, keepdims=True)

    for p in t_peers:
        t_copy(p, p).wait_recv()
    summed = tbuf[0]
    for i in range(1, ntp):
        summed += tbuf[i]
    summed = (summed + pltpu.roll(summed, HD, 1))[:, 0:HD]
    dqgain_ref[...] = summed
    dkgain_ref[...] = summed * qgain_ref[...] / kgain_ref[...]

    for tile in range(TILES):
        for kind in range(4):
            halo_copy(kind, tile).wait_send()
        stat_copy(tile).wait_send()
    for p in y_peers:
        y_copy(p, y).wait_send()
    for p in z_peers:
        z_copy(p, z).wait_send()
    for p in t_peers:
        t_copy(p, t_me).wait_send()


def per_device(sizes, query, key, value, out_grad, query_gain, key_gain, rel_bias):
    nz, ny, nx, nc = sizes
    vmem = pl.BlockSpec(memory_space=pltpu.VMEM)
    dma = pltpu.SemaphoreType.DMA
    big = jax.ShapeDtypeStruct((ROWS, LANES), bf16)
    gain = jax.ShapeDtypeStruct((1, HD), f32)
    outs = pl.pallas_call(
        functools.partial(body, sizes),
        out_shape=(big, big, big, gain, gain, jax.ShapeDtypeStruct(rel_bias.shape, f32)),
        in_specs=[vmem] * 7,
        out_specs=(vmem,) * 6,
        scratch_shapes=[
            pltpu.VMEM((ROWS, LANES), bf16),
            pltpu.VMEM((ROWS, LANES), bf16),
            pltpu.VMEM((ROWS, LANES), bf16),
            pltpu.VMEM((ROWS, LANES), bf16),
            pltpu.VMEM((TILES, 8, WIDE), f32),
            pltpu.VMEM((TILES, 8, WIDE), f32),
            pltpu.VMEM((ROWS, LANES), f32),
            pltpu.VMEM((ROWS, LANES), f32),
            pltpu.VMEM((ROWS, LANES), bf16),
            pltpu.VMEM((ROWS, LANES), bf16),
            pltpu.VMEM((TILES * WIDE, LANES), bf16),
            pltpu.VMEM((TILES * WIDE, LANES), bf16),
            pltpu.VMEM((TILES * WIDE, LANES), bf16),
            pltpu.VMEM((TILES * WIDE, LANES), bf16),
            pltpu.VMEM((TILES, (TILES + 1) * TILE, WIDE), f32),
            pltpu.VMEM((TILES, (TILES + 1) * TILE, WIDE), f32),
            pltpu.VMEM((ROWS, TILES * WIDE), f32),
            pltpu.VMEM((ROWS, TILES * WIDE), f32),
            pltpu.VMEM((ROWS, TILES * WIDE), bf16),
            pltpu.VMEM((ROWS, TILES * WIDE), bf16),
            pltpu.VMEM((ROWS, TILES * WIDE), bf16),
            pltpu.VMEM((ROWS, TILES * WIDE), bf16),
            pltpu.VMEM((ny, 4, LANES), f32),
            pltpu.VMEM((nz, 4, LANES), f32),
            pltpu.VMEM((nx * nc, 1, LANES), f32),
            dma((4, TILES)),
            dma((4, TILES)),
            dma((TILES,)),
            dma((TILES,)),
            dma((ny,)),
            dma((ny,)),
            dma((nz,)),
            dma((nz,)),
            dma((nx * nc,)),
            dma((nx * nc,)),
        ],
        compiler_params=pltpu.CompilerParams(collective_id=0, has_side_effects=True),
        name="segment_backward",
    )(query, key, value, out_grad, query_gain.reshape(1, HD), key_gain.reshape(1, HD), rel_bias)
    return (*outs[:3], outs[3].reshape(HD), outs[4].reshape(HD), outs[5])


def solution(mesh):
    sizes = mesh_sizes(mesh)
    torus = Mesh(mesh.devices.reshape(sizes), ("z", "y", "x", "c"))
    return jax.shard_map(
        functools.partial(per_device, sizes),
        mesh=torus,
        in_specs=(P(SP, TP), P(SP, TP), P(SP, TP), P(SP, TP), P(), P(), P(TP, None)),
        out_specs=(P(SP, TP), P(SP, TP), P(SP, TP), P(), P(), P(TP, None)),
        check_vma=False,
    )


def mesh_sizes(mesh):
    return (16, 8, 4, 2)
```

time: 171 us -> 56 us (0.33)
  blocking collectives: 77.8 us -> 0 us
  Pallas kernels: 0 us -> 50.3 us
  local copies, waits for them, and re-layouts: 45.4 us -> 4.82 us
  other arithmetic: 20.6 us -> 0 us
  matrix products: 10.7 us -> 0 us
  starting transfers between devices: 9.81 us -> 0 us
  loops' own time: 3.06 us -> 0 us
  waiting for transfers between devices: 2.05 us -> 0 us
    psum x4 -> x0, blocking collectives: 77.8 us -> none  [over_axes(): return functools.reduce(lax.psum, axes, shard)]
    pallas_call x0 -> x1, Pallas kernels: none -> 50.3 us  [per_device(): pl.pallas_call(functools.partial(body, sizes), out_shape=(big, big, big,...]
    reshape x6 -> x0, local copies, waits for them, and re-layouts: 21.7 us -> none  [the longest x2 8.1 us: tap_totals(): flattened = jnp.pad(widened.reshape(-1), (0, block))]
    dot_general x12 -> x0, matrix products: 10.7 us -> none  [the longest x2 4.14 us: block_gradients(): jnp.dot(query_block, key_block.T, preferred_element_type=jnp.float32)]
    ppermute x4 -> x0, starting transfers between devices: 9.81 us -> none  [shifted(): return lax.ppermute(block, axis, route)]
    pad x2 -> x0, other arithmetic: 6.01 us -> none  [tap_totals(): flattened = jnp.pad(widened.reshape(-1), (0, block))]
    convert_element_type x6 -> x0, other arithmetic: 5.58 us -> none  [the longest x2 2.59 us: block_gradients(): attention_low = attention.astype(jnp.bfloat16)]
    reduce_sum x12 -> x0, other arithmetic: 4.84 us -> none  [the longest x2 2.53 us: norm_backward(): jnp.sum(grad_hat * unit_rows, axis=(0, 1))]
  transfers between devices with their start and end apart: 4 -> 0, of which waited for: 2 -> 0; matrix products, arithmetic and copies ran while one was open for 7% -> 0% of each run, Pallas kernels for 0% -> 0%
where the time goes in v1:
time: 56 us; the launch traced here: 55.8 us
  Pallas kernels  50.3 us (90%)
  local copies, waits for them, and re-layouts  4.82 us (9%)
  between operations  0.66 us (1%)
    pallas_call x1, Pallas kernels, per_device(): pl.pallas_call(functools.partial(body, sizes), out_shape=(big, big, big,...  50.3 us
    unnamed x16, local copies, waits for them, and re-layouts  4.82 us

profile of v1, /device:TPU:1, one launch (start us, length us, event | category | flops | bytes accessed | tf_op | source)
XLA Modules:
  0.0 55.8 jit_solution(8197285017179651550)
XLA Ops:
  0.6 50.3 %segment_backward.1 = (bf16[512,128]{1,0:T(8,128)(2,1)}, bf16[512,128]{1,0:T(8,128)(2,1)}, bf16[512,128]{1,0:T(8,128)(2,1)}, f32[1,64]{1,0:T(1,128)}, f32[1,64]{1,0:T(1,128)}, /*index=5*/f32[2,129]{1,0:T(2,128)}) custom-call(bf16[512,128]{1,0:T(8,128)(2,1)} %q_ref.1, bf16[512,128]{1,0:T(8,128)(2,1)} %k_ref.1, bf16[512,128]{1,0:T(8,128)(2,1)} %v_ref.1, ...), custom_call_target="tpu_custom_call" | custom-call | tf_op jit(solution)/shard_map/segment_backward/pallas_call | solution.py:428
  50.9 0.0 copy-start.1
  50.9 1.6 %copy.19 = bf16[512,128]{1,0:T(8,128)(2,1)} copy(bf16[512,128]{1,0:T(8,128)(2,1)} %get-tuple-element.24) | data formatting | bytes 262144
  52.5 0.0 copy-done.1
  52.5 0.0 copy-start
  52.5 0.7 %copy.20 = bf16[512,128]{1,0:T(8,128)(2,1)} copy(bf16[512,128]{1,0:T(8,128)(2,1)S(1)} %copy-done.1) | data formatting | bytes 262144
  53.2 0.3 copy-done
  53.5 0.0 copy-start.4
  53.5 0.0 copy-start.3
  53.5 0.7 %copy.21 = bf16[512,128]{1,0:T(8,128)(2,1)} copy(bf16[512,128]{1,0:T(8,128)(2,1)S(1)} %copy-done) | data formatting | bytes 262144
  54.1 0.0 copy-done.4
  54.1 0.0 copy-start.2
  54.1 0.5 copy.22
  54.7 0.0 copy-done.3
  54.7 0.5 copy.23
  55.2 0.0 copy-done.2
  55.2 0.6 %copy.24 = f32[2,129]{1,0:T(2,128)} copy(f32[2,129]{1,0:T(2,128)S(1)} %copy-done.2) | data formatting | bytes 2064
Async XLA Ops:
  50.9 1.6 %copy-start.1 = (bf16[512,128]{1,0:T(8,128)(2,1)S(1)}, bf16[512,128]{1,0:T(8,128)(2,1)}, u32[]{:S(2)}) copy-start(bf16[512,128]{1,0:T(8,128)(2,1)} %get-tuple-element.25) | copy-start | bytes 393220
  52.5 1.0 %copy-start = (bf16[512,128]{1,0:T(8,128)(2,1)S(1)}, bf16[512,128]{1,0:T(8,128)(2,1)}, u32[]{:S(2)}) copy-start(bf16[512,128]{1,0:T(8,128)(2,1)} %get-tuple-element.26) | copy-start | bytes 393220
  53.5 0.7 %copy-start.4 = (f32[1,64]{1,0:T(1,128)S(1)}, f32[1,64]{1,0:T(1,128)}, u32[]{:S(2)}) copy-start(f32[1,64]{1,0:T(1,128)} %get-tuple-element.15) | copy-start | bytes 772
  53.5 1.2 %copy-start.3 = (f32[1,64]{1,0:T(1,128)S(1)}, f32[1,64]{1,0:T(1,128)}, u32[]{:S(2)}) copy-start(f32[1,64]{1,0:T(1,128)} %get-tuple-element.16) | copy-start | bytes 772
  54.1 1.0 %copy-start.2 = (f32[2,129]{1,0:T(2,128)S(1)}, f32[2,129]{1,0:T(2,128)}, u32[]{:S(2)}) copy-start(f32[2,129]{1,0:T(2,128)} %get-tuple-element.29) | copy-start | bytes 3100

commit v2 on v1

--- a/solution.py
+++ b/solution.py
@@ -85,6 +85,19 @@
 
 def body(
     sizes,
+    q_hbm,
+    k_hbm,
+    v_hbm,
+    g_hbm,
+    qgain_hbm,
+    kgain_hbm,
+    bias_hbm,
+    dq_ref,
+    dk_ref,
+    dv_ref,
+    dqgain_ref,
+    dkgain_ref,
+    dbias_ref,
     q_ref,
     k_ref,
     v_ref,
@@ -92,12 +105,6 @@
     qgain_ref,
     kgain_ref,
     bias_ref,
-    dq_ref,
-    dk_ref,
-    dv_ref,
-    dqgain_ref,
-    dkgain_ref,
-    dbias_ref,
     hk_ref,
     hv_ref,
     nq_ref,
@@ -106,6 +113,7 @@
     recv_stat,
     unit_q,
     scale_q,
+    grad_q,
     khat_ref,
     hkhat_ref,
     qm_ref,
@@ -120,45 +128,78 @@
     sown_ref,
     pn_ref,
     sn_ref,
-    ybuf,
-    zbuf,
-    tbuf,
+    abuf,
+    again,
+    asend,
+    bbuf,
+    bgain,
+    bsend,
+    load_sem,
     halo_send,
     halo_recv,
     stat_ssem,
     stat_rsem,
-    y_ssem,
-    y_rsem,
-    z_ssem,
-    z_rsem,
-    t_ssem,
-    t_rsem,
+    a_ssem,
+    a_rsem,
+    b_ssem,
+    b_rsem,
+    level_1,
+    level_2,
+    level_3,
+    x_ready,
+    c_ready,
 ):
     nz, ny, nx, nc = sizes
-    nsp, ntp = nz * ny, nx * nc
+    nsp = nz * ny
     z, y, x, c = (lax.axis_index(a) for a in ("z", "y", "x", "c"))
     sp = z * ny + y
     after, before = lax.rem(sp + 1, nsp), lax.rem(sp + nsp - 1, nsp)
-    t_me = x * nc + c
 
     def at_sp(i):
         return {"z": i // ny, "y": lax.rem(i, ny)}
 
-    def at_tp(i):
-        return {"x": i // nc, "c": lax.rem(i, nc)}
-
-    y_peers = [lax.rem(y + d, ny) for d in range(1, ny)]
-    z_peers = [lax.rem(z + d, nz) for d in range(1, nz)]
-    t_peers = [lax.rem(t_me + d, ntp) for d in range(1, ntp)]
+    def both_ways(name, place, size, distance):
+        return [
+            {name: lax.rem(place + distance, size)},
+            {name: lax.rem(place + (distance // size + 1) * size - distance, size)},
+        ]
+
+    def tell(sem, targets):
+        for target in targets:
+            pl.semaphore_signal(sem, inc=1, device_id=target, device_id_type=MESH)
+
+    axes = both_ways("z", z, nz, 1) + both_ways("y", y, ny, 1)
+    if nx > 1:
+        axes += both_ways("x", x, nx, 1)
+    partner = [{"c": lax.rem(c + d, nc)} for d in range(1, nc)]
+    x_peers = [{"x": lax.rem(x + d, nx)} for d in range(1, nx)]
+    two_away = both_ways("z", z, nz, 2) + both_ways("y", y, ny, 2)
+    four_away = both_ways("z", z, nz, 4)
 
     barrier = pltpu.get_barrier_semaphore()
-    targets = [at_sp(after), at_sp(before)]
-    targets += [{"y": p} for p in y_peers]
-    targets += [{"z": p} for p in z_peers]
-    targets += [at_tp(p) for p in t_peers]
-    for target in targets:
-        pl.semaphore_signal(barrier, inc=1, device_id=target, device_id_type=MESH)
-    pl.semaphore_wait(barrier, len(targets))
+    neighbours = [at_sp(after), at_sp(before)] + axes + partner
+    tell(barrier, neighbours)
+
+    loads = [
+        pltpu.make_async_copy(src, dst, load_sem.at[i])
+        for i, (src, dst) in enumerate(
+            (
+                (k_hbm, k_ref),
+                (v_hbm, v_ref),
+                (q_hbm, q_ref),
+                (g_hbm, g_ref),
+                (qgain_hbm, qgain_ref),
+                (kgain_hbm, kgain_ref),
+                (bias_hbm, bias_ref),
+            )
+        )
+    ]
+    for load in loads:
+        load.start()
+    pl.semaphore_wait(barrier, len(neighbours))
+    tell(level_1, axes)
+    for load in loads:
+        load.wait()
 
     def halo_copy(kind, tile):
         src, dst, to = (
@@ -221,6 +262,8 @@
         qm_ref[t * WIDE : (t + 1) * WIDE] = both_heads(hat)
         gm_ref[t * WIDE : (t + 1) * WIDE] = both_heads(g_ref[rows])
     khat_ref[...] = normalize(k_ref[...], kgain, ones)[2]
+    pl.semaphore_wait(level_1, len(axes))
+    tell(level_2, two_away)
 
     nt = ((1,), (1,))
     l_parts, n_parts = [], []
@@ -241,6 +284,9 @@
             n_sum += jnp.sum(e * d[part], axis=0, keepdims=True)
         l_parts.append(l_sum)
         n_parts.append(n_sum)
+    pl.semaphore_wait(level_2, len(two_away))
+    tell(level_3, four_away)
+    tell(x_ready, x_peers)
 
     def stat_copy(t):
         return pltpu.make_async_remote_copy(
@@ -284,10 +330,7 @@
         total += jnp.sum(grad, axis=0, keepdims=True)
         own = (TILES - t) * TILE
         near_sum += grad[TILES * TILE :]
-        if t > 0:
-            mid_sum += grad[(TILES - 1) * TILE : TILES * TILE]
-        else:
-            mid_sum += grad[(TILES - 1) * TILE : TILES * TILE]
+        mid_sum += grad[(TILES - 1) * TILE : TILES * TILE]
         low = grad.astype(bf16)
         pown_ref[0 : (t + 1) * TILE, cols] = prob[own:].astype(bf16)
         sown_ref[0 : (t + 1) * TILE, cols] = low[own:]
@@ -295,49 +338,38 @@
         dq_t = dot(keys, low, ((0,), (0,)))
         dq_t = jnp.concatenate([dq_t[0:HD, 0:TILE], dq_t[HD:, TILE:]], axis=0) * SCALE
         grad_hat = dq_t.T
-        unit = unit_q[rows]
-        gain_sum += jnp.sum(grad_hat * unit, axis=0, keepdims=True)
-        dq_ref[rows] = norm_backward(grad_hat, unit, scale_q[rows], qgain, ones).astype(bf16)
+        grad_q[rows] = grad_hat
+        gain_sum += jnp.sum(grad_hat * unit_q[rows], axis=0, keepdims=True)
 
     diagonals = jnp.where(both_reached, near_sum, mid_sum)
     taps = [diagonal_sums(diagonals[:, h * TILE : (h + 1) * TILE]) for h in range(2)]
     sums = [jnp.sum(total[:, h * TILE : (h + 1) * TILE], axis=1, keepdims=True) for h in range(2)]
     lane = iota((1, LANES), 1)
     sums = jnp.where(lane < HD, sums[0], sums[1])
-    ybuf[y] = jnp.concatenate([taps[0], taps[1], gain_sum, sums], axis=0)
-
-    def y_copy(peer, slot):
+    abuf[y] = jnp.concatenate([taps[0], taps[1], sums, gain_sum], axis=0)
+    asend[...] = gain_sum
+
+    a_offsets = [(dy, dx) for dx in range(nx) for dy in range(ny) if (dy, dx) != (0, 0)]
+
+    def a_copy(dy, dx, arriving=False):
+        to_y, to_x = lax.rem(y + dy, ny), lax.rem(x + dx, nx)
+        source_y, source_x = (to_y, to_x) if arriving else (y, x)
+        slot = source_x * ny + source_y
         return pltpu.make_async_remote_copy(
-            src_ref=ybuf.at[slot],
-            dst_ref=ybuf.at[slot],
-            send_sem=y_ssem.at[peer],
-            recv_sem=y_rsem.at[slot],
-            device_id={"y": peer},
+            src_ref=abuf.at[source_y] if dx == 0 else asend,
+            dst_ref=abuf.at[source_y] if dx == 0 else again.at[slot],
+            send_sem=a_ssem.at[to_x * ny + to_y],
+            recv_sem=a_rsem.at[slot],
+            device_id={"y": to_y, "x": to_x},
             device_id_type=MESH,
         )
 
-    def z_copy(peer, slot):
-        return pltpu.make_async_remote_copy(
-            src_ref=zbuf.at[slot],
-            dst_ref=zbuf.at[slot],
-            send_sem=z_ssem.at[peer],
-            recv_sem=z_rsem.at[slot],
-            device_id={"z": peer},
-            device_id_type=MESH,
-        )
-
-    def t_copy(peer, slot):
-        return pltpu.make_async_remote_copy(
-            src_ref=tbuf.at[slot],
-            dst_ref=tbuf.at[slot],
-            send_sem=t_ssem.at[peer],
-            recv_sem=t_rsem.at[slot],
-            device_id=at_tp(peer),
-            device_id_type=MESH,
-        )
-
-    for p in y_peers:
-        y_copy(p, y).start()
+    if x_peers:
+        pl.semaphore_wait(x_ready, len(x_peers))
+    for dy, dx in a_offsets:
+        a_copy(dy, dx).start()
+    pl.semaphore_wait(level_3, len(four_away))
+    tell(c_ready, partner)
 
     for t in reversed(range(TILES)):
         rows = slice(t * TILE, (t + 1) * TILE)
@@ -356,22 +388,50 @@
             )
             dn_ref[rows, cols] = d[part]
 
-    for p in y_peers:
-        y_copy(p, p).wait_recv()
-    summed = ybuf[0]
+    for dy, dx in a_offsets:
+        a_copy(dy, dx, arriving=True).wait_recv()
+    block = abuf[0]
     for i in range(1, ny):
-        summed += ybuf[i]
-    zbuf[z] = summed
-    for p in z_peers:
-        z_copy(p, z).start()
+        block += abuf[i]
+    for i in range(ny):
+        again[x * ny + i] = abuf[i, 3:4]
+    gain_sum = again[0]
+    for i in range(1, nx * ny):
+        gain_sum += again[i]
+    bbuf[z] = jnp.concatenate([block[0:3], gain_sum], axis=0)
+    bsend[...] = gain_sum
+
+    b_offsets = [(dz, dc) for dc in range(nc) for dz in range(nz) if (dz, dc) != (0, 0)]
+
+    def b_copy(dz, dc, arriving=False):
+        to_z, to_c = lax.rem(z + dz, nz), lax.rem(c + dc, nc)
+        source_z, source_c = (to_z, to_c) if arriving else (z, c)
+        slot = source_c * nz + source_z
+        return pltpu.make_async_remote_copy(
+            src_ref=bbuf.at[source_z] if dc == 0 else bsend,
+            dst_ref=bbuf.at[source_z] if dc == 0 else bgain.at[slot],
+            send_sem=b_ssem.at[to_c * nz + to_z],
+            recv_sem=b_rsem.at[slot],
+            device_id={"z": to_z, "c": to_c},
+            device_id_type=MESH,
+        )
+
+    if partner:
+        pl.semaphore_wait(c_ready, len(partner))
+    for dz, dc in b_offsets:
+        b_copy(dz, dc).start()
 
     for t in reversed(range(TILES)):
+        rows = slice(t * TILE, (t + 1) * TILE)
         cols = slice(t * WIDE, (t + 1) * WIDE)
         stat_copy(t).wait_recv()
         inv, delta = recv_stat[t, 0:1], recv_stat[t, 1:2]
         prob = en_ref[t * TILE :, cols] * inv
         pn_ref[t * TILE :, cols] = prob.astype(bf16)
         sn_ref[t * TILE :, cols] = (prob * (dn_ref[t * TILE :, cols] - delta)).astype(bf16)
+        dq_ref[rows] = norm_backward(
+            grad_q[rows], unit_q[rows], scale_q[rows], qgain, ones
+        ).astype(bf16)
 
     unit_k, scale_k, _ = normalize(k_ref[...], kgain, ones)
     for ck in range(TILES):
@@ -384,92 +444,101 @@
             dk * SCALE, unit_k[rows], scale_k[rows], kgain, ones
         ).astype(bf16)
 
-    for p in z_peers:
-        z_copy(p, p).wait_recv()
-    summed = zbuf[0]
-    for i in range(1, nz):
-        summed += zbuf[i]
-    tbuf[t_me] = summed[2:3]
-    for p in t_peers:
-        t_copy(p, t_me).start()
-    rest = [summed[3:4, h * HD : h * HD + 1] for h in range(2)]
-    for h in range(2):
-        taps = summed[h : h + 1]
-        dbias_ref[h : h + 1, 0:LANES] = taps
-        dbias_ref[h : h + 1, LANES : LANES + 1] = rest[h] - jnp.sum(taps, axis=1, keepdims=True)
-
-    for p in t_peers:
-        t_copy(p, p).wait_recv()
-    summed = tbuf[0]
-    for i in range(1, ntp):
-        summed += tbuf[i]
-    summed = (summed + pltpu.roll(summed, HD, 1))[:, 0:HD]
-    dqgain_ref[...] = summed
-    dkgain_ref[...] = summed * qgain_ref[...] / kgain_ref[...]
-
     for tile in range(TILES):
         for kind in range(4):
             halo_copy(kind, tile).wait_send()
         stat_copy(tile).wait_send()
-    for p in y_peers:
-        y_copy(p, y).wait_send()
-    for p in z_peers:
-        z_copy(p, z).wait_send()
-    for p in t_peers:
-        t_copy(p, t_me).wait_send()
+    for dy, dx in a_offsets:
+        a_copy(dy, dx).wait_send()
+
+    for dz, dc in b_offsets:
+        b_copy(dz, dc, arriving=True).wait_recv()
+    block = bbuf[0]
+    for i in range(1, nz):
+        block += bbuf[i]
+    for i in range(nz):
+        bgain[c * nz + i] = bbuf[i, 3:4]
+    gain_sum = bgain[0]
+    for i in range(1, nc * nz):
+        gain_sum += bgain[i]
+    for h in range(2):
+        taps = block[h : h + 1]
+        rest = block[2:3, h * HD : h * HD + 1] - jnp.sum(taps, axis=1, keepdims=True)
+        dbias_ref[h : h + 1, 0:LANES] = taps
+        dbias_ref[h : h + 1, LANES : LANES + 1] = rest
+    gain_sum = (gain_sum + pltpu.roll(gain_sum, HD, 1))[:, 0:HD]
+    dqgain_ref[...] = gain_sum
+    dkgain_ref[...] = gain_sum * qgain_ref[...] / kgain_ref[...]
+    for dz, dc in b_offsets:
+        b_copy(dz, dc).wait_send()
+
+
+def flush(*refs):
+    count = len(refs) // 2
+    sems = refs[-1]
+    copies = [
+        pltpu.make_async_copy(refs[i], refs[count + i], sems.at[i]) for i in range(count)
+    ]
+    for copy in copies:
+        copy.start()
+    for copy in copies:
+        copy.wait()
 
 
 def per_device(sizes, query, key, value, out_grad, query_gain, key_gain, rel_bias):
     nz, ny, nx, nc = sizes
     vmem = pl.BlockSpec(memory_space=pltpu.VMEM)
+    hbm = pl.BlockSpec(memory_space=pl.ANY)
     dma = pltpu.SemaphoreType.DMA
-    big = jax.ShapeDtypeStruct((ROWS, LANES), bf16)
-    gain = jax.ShapeDtypeStruct((1, HD), f32)
+    regular = pltpu.SemaphoreType.REGULAR
+    shapes = (((ROWS, LANES), bf16),) * 3 + (((1, HD), f32),) * 2 + ((rel_bias.shape, f32),)
+    tile_rows, wide_rows = (ROWS, LANES), (TILES * WIDE, LANES)
+    square = (ROWS, TILES * WIDE)
     outs = pl.pallas_call(
         functools.partial(body, sizes),
-        out_shape=(big, big, big, gain, gain, jax.ShapeDtypeStruct(rel_bias.shape, f32)),
-        in_specs=[vmem] * 7,
+        out_shape=tuple(pltpu.VMEM(*s) for s in shapes),
+        in_specs=[hbm] * 7,
         out_specs=(vmem,) * 6,
         scratch_shapes=[
-            pltpu.VMEM((ROWS, LANES), bf16),
-            pltpu.VMEM((ROWS, LANES), bf16),
-            pltpu.VMEM((ROWS, LANES), bf16),
-            pltpu.VMEM((ROWS, LANES), bf16),
-            pltpu.VMEM((TILES, 8, WIDE), f32),
-            pltpu.VMEM((TILES, 8, WIDE), f32),
-            pltpu.VMEM((ROWS, LANES), f32),
-            pltpu.VMEM((ROWS, LANES), f32),
-            pltpu.VMEM((ROWS, LANES), bf16),
-            pltpu.VMEM((ROWS, LANES), bf16),
-            pltpu.VMEM((TILES * WIDE, LANES), bf16),
-            pltpu.VMEM((TILES * WIDE, LANES), bf16),
-            pltpu.VMEM((TILES * WIDE, LANES), bf16),
-            pltpu.VMEM((TILES * WIDE, LANES), bf16),
-            pltpu.VMEM((TILES, (TILES + 1) * TILE, WIDE), f32),
-            pltpu.VMEM((TILES, (TILES + 1) * TILE, WIDE), f32),
-            pltpu.VMEM((ROWS, TILES * WIDE), f32),
-            pltpu.VMEM((ROWS, TILES * WIDE), f32),
-            pltpu.VMEM((ROWS, TILES * WIDE), bf16),
-            pltpu.VMEM((ROWS, TILES * WIDE), bf16),
-            pltpu.VMEM((ROWS, TILES * WIDE), bf16),
-            pltpu.VMEM((ROWS, TILES * WIDE), bf16),
+            *[pltpu.VMEM(tile_rows, bf16)] * 4,
+            *[pltpu.VMEM((1, HD), f32)] * 2,
+            pltpu.VMEM(rel_bias.shape, f32),
+            *[pltpu.VMEM(tile_rows, bf16)] * 4,
+            *[pltpu.VMEM((TILES, 8, WIDE), f32)] * 2,
+            *[pltpu.VMEM(tile_rows, f32)] * 3,
+            *[pltpu.VMEM(tile_rows, bf16)] * 2,
+            *[pltpu.VMEM(wide_rows, bf16)] * 4,
+            *[pltpu.VMEM((TILES, (TILES + 1) * TILE, WIDE), f32)] * 2,
+            *[pltpu.VMEM(square, f32)] * 2,
+            *[pltpu.VMEM(square, bf16)] * 4,
             pltpu.VMEM((ny, 4, LANES), f32),
+            pltpu.VMEM((nx * ny, 1, LANES), f32),
+            pltpu.VMEM((1, LANES), f32),
             pltpu.VMEM((nz, 4, LANES), f32),
-            pltpu.VMEM((nx * nc, 1, LANES), f32),
+            pltpu.VMEM((nc * nz, 1, LANES), f32),
+            pltpu.VMEM((1, LANES), f32),
+            dma((7,)),
             dma((4, TILES)),
             dma((4, TILES)),
             dma((TILES,)),
             dma((TILES,)),
-            dma((ny,)),
-            dma((ny,)),
-            dma((nz,)),
-            dma((nz,)),
-            dma((nx * nc,)),
-            dma((nx * nc,)),
+            dma((nx * ny,)),
+            dma((nx * ny,)),
+            dma((nc * nz,)),
+            dma((nc * nz,)),
+            *[regular] * 5,
         ],
         compiler_params=pltpu.CompilerParams(collective_id=0, has_side_effects=True),
         name="segment_backward",
     )(query, key, value, out_grad, query_gain.reshape(1, HD), key_gain.reshape(1, HD), rel_bias)
+    outs = pl.pallas_call(
+        flush,
+        out_shape=tuple(jax.ShapeDtypeStruct(*s) for s in shapes),
+        in_specs=[vmem] * 6,
+        out_specs=(hbm,) * 6,
+        scratch_shapes=[dma((6,))],
+        name="flush",
+    )(*(pltpu.with_memory_space_constraint(o, pltpu.VMEM) for o in outs))
     return (*outs[:3], outs[3].reshape(HD), outs[4].reshape(HD), outs[5])
 
 

time: 56 us -> 45.2 us (0.81)
  Pallas kernels: 50.3 us -> 44.5 us
  local copies, waits for them, and re-layouts: 4.82 us -> 0 us
    pallas_call x1 -> x2, Pallas kernels: 50.3 us -> 44.5 us  [the longest x1 43.7 us: per_device(): pl.pallas_call(functools.partial(body, sizes), out_shape=tuple((pltpu.VME...]
    unnamed x16 -> x0, local copies, waits for them, and re-layouts: 4.82 us -> none
where the time goes in v2:
time: 45.2 us; the launch traced here: 45.1 us
  Pallas kernels  44.5 us (98%)
  between operations  0.64 us (1%)
    pallas_call x1, Pallas kernels, per_device(): pl.pallas_call(functools.partial(body, sizes), out_shape=tuple((pltpu.VME...  43.7 us

profile of v2, /device:TPU:1, one launch (start us, length us, event | category | flops | bytes accessed | tf_op | source)
XLA Modules:
  0.0 45.1 jit_solution(7486458289390757499)
XLA Ops:
  0.6 43.7 %segment_backward.1 = (bf16[512,128]{1,0:T(8,128)(2,1)S(1)}, bf16[512,128]{1,0:T(8,128)(2,1)S(1)}, bf16[512,128]{1,0:T(8,128)(2,1)S(1)}, f32[1,64]{1,0:T(1,128)S...) custom-call(bf16[512,128]{1,0:T(8,128)(2,1)} %q_hbm.1, bf16[512,128]{1,0:T(8,128)(2,1)} %k_hbm.1, bf16[512,128]{1,0:T(8,128)(2,1)} %v_hbm.1, ...), custom_call_target="tpu_custom_call" | custom-call | tf_op jit(solution)/shard_map/segment_backward/pallas_call | solution.py:497
  44.3 0.8 %flush.1 = (bf16[512,128]{1,0:T(8,128)(2,1)}, bf16[512,128]{1,0:T(8,128)(2,1)}, bf16[512,128]{1,0:T(8,128)(2,1)}, f32[1,64]{1,0:T(1,128)}, f32[1,64]{1,0:T(1,128)}, /*index=5*/f32[2,129]{1,0:T(2,128)}) custom-call(bf16[512,128]{1,0:T(8,128)(2,1)S(1)} %get-tuple-element.18.refs_0_, bf16[512,128]{1,0:T(8,128)(2,1)S(1)} %get-tuple-element.19.refs_1_, ...), custom_call_target="tpu_custom_call" | custom-call | tf_op jit(solution)/shard_map/flush/pallas_call | solution.py:534

commit v3 on v2

v3 whole, which is shorter than its diff:
```python
import functools

import jax
import jax.numpy as jnp
from jax import lax
from jax.experimental import pallas as pl
from jax.experimental.pallas import tpu as pltpu
from jax.sharding import Mesh
from jax.sharding import PartitionSpec as P

SP = ("z", "y")
TP = ("x", "c")
MESH = pl.DeviceIdType.MESH

ROWS = 512
TILE = 128
TILES = ROWS // TILE
LANES = 128
HD = 64
WIDE = 2 * TILE
EPS = 1e-06
LOG2E = 1.4426950408889634
SCALE = HD**-0.5
OFF = -1e30

f32 = jnp.float32
bf16 = jnp.bfloat16


def dot(a, b, dims=((1,), (0,))):
    return lax.dot_general(a, b, (dims, ((), ())), preferred_element_type=f32)


def iota(shape, axis):
    return lax.broadcasted_iota(jnp.int32, shape, axis)


def head_sums(x, ones):
    high = x.astype(bf16)
    low = (x - high.astype(f32)).astype(bf16)
    return dot(high, ones) + dot(low, ones)


def normalize(x, gain, ones):
    wide = x.astype(f32)
    scale = lax.rsqrt(head_sums(wide * wide, ones) * (1.0 / HD) + EPS)
    unit = wide * scale
    return unit, scale, (unit * gain).astype(bf16)


def norm_backward(grad_hat, unit, scale, gain, ones):
    grad_unit = grad_hat * gain
    inner = head_sums(grad_unit * unit, ones) * (1.0 / HD)
    return scale * (grad_unit - unit * inner)


def shifted_rows(row):
    rows = jnp.broadcast_to(row, (TILE, LANES))
    return pltpu.roll(rows, 0, 1, stride=1, stride_axis=0)


def diagonal_sums(block):
    parts = [block[0:8]]
    for i in range(8, TILE, 8):
        parts.append(pltpu.roll(block[i : i + 8], LANES - i, 1))
    while len(parts) > 1:
        parts = [parts[i] + parts[i + 1] for i in range(0, len(parts), 2)]
    block = parts[0]
    index = iota((8, LANES), 0)
    for bit in (1, 2, 4):
        block = jnp.where((index & bit) != 0, pltpu.roll(block, LANES - bit, 1), block)
    return jnp.sum(block, axis=0, keepdims=True)


def both_heads(a):
    first = iota((TILE, LANES), 1) < HD
    zero = jnp.zeros((), a.dtype)
    return jnp.concatenate([jnp.where(first, a, zero), jnp.where(first, zero, a)], axis=0)


def body(
    sizes,
    q_hbm,
    k_hbm,
    v_hbm,
    g_hbm,
    qgain_hbm,
    kgain_hbm,
    bias_hbm,
    dq_ref,
    dk_ref,
    dv_ref,
    dqgain_ref,
    dkgain_ref,
    dbias_ref,
    qgain_ref,
    kgain_ref,
    bias_ref,
    kv_ref,
    hkv_ref,
    qg_ref,
    nqg_ref,
    send_stat,
    recv_stat,
    unit_q,
    scale_q,
    unit_k,
    scale_k,
    dk_acc,
    khat_ref,
    hkhat_ref,
    v_ref,
    qm_ref,
    gm_ref,
    qmn_ref,
    gmn_ref,
    e_ref,
    d_ref,
    low_ref,
    en_ref,
    dn_ref,
    pown_ref,
    pn_ref,
    sn_ref,
    abuf,
    again,
    asend,
    bbuf,
    bgain,
    bsend,
    load_sem,
    halo_recv,
    halo_send,
    stat_sem,
    a_sem,
    b_sem,
    level,
):
    nz, ny, nx, nc = sizes
    nsp = nz * ny
    z, y, x, c = (lax.axis_index(a) for a in ("z", "y", "x", "c"))
    sp = z * ny + y
    after, before = lax.rem(sp + 1, nsp), lax.rem(sp + nsp - 1, nsp)

    def at_sp(i):
        return {"z": i // ny, "y": lax.rem(i, ny)}

    def both_ways(name, place, size, distance):
        return [
            {name: lax.rem(place + distance, size)},
            {name: lax.rem(place + (distance // size + 1) * size - distance, size)},
        ]

    def tell(sem, targets):
        for target in targets:
            pl.semaphore_signal(sem, inc=1, device_id=target, device_id_type=MESH)

    def wait_bytes(ref, sem):
        pltpu.make_async_copy(ref, ref, sem).wait()

    axes = both_ways("z", z, nz, 1) + both_ways("y", y, ny, 1)
    if nx > 1:
        axes += both_ways("x", x, nx, 1)
    partner = [{"c": lax.rem(c + d, nc)} for d in range(1, nc)]
    x_peers = [{"x": lax.rem(x + d, nx)} for d in range(1, nx)]
    two_away = both_ways("z", z, nz, 2) + both_ways("y", y, ny, 2)
    four_away = both_ways("z", z, nz, 4)
    level_1, level_2, level_3, x_ready, c_ready = (level.at[i] for i in range(5))

    barrier = pltpu.get_barrier_semaphore()
    neighbours = [at_sp(after), at_sp(before)] + axes + partner
    tell(barrier, neighbours)

    tiles = [slice(t * TILE, (t + 1) * TILE) for t in range(TILES)]
    wides = [slice(t * WIDE, (t + 1) * WIDE) for t in range(TILES)]
    for first, second, ref, sem in ((k_hbm, v_hbm, kv_ref, 0), (q_hbm, g_hbm, qg_ref, 1)):
        for t in reversed(range(TILES)):
            for half, src in enumerate((first, second)):
                dst = ref.at[t, pl.ds(half * TILE, TILE)]
                pltpu.make_async_copy(src.at[tiles[t]], dst, load_sem.at[sem]).start()
    small = [
        pltpu.make_async_copy(src, dst, load_sem.at[2 + i])
        for i, (src, dst) in enumerate(
            ((qgain_hbm, qgain_ref), (kgain_hbm, kgain_ref), (bias_hbm, bias_ref))
        )
    ]
    for load in small:
        load.start()
    pl.semaphore_wait(barrier, len(neighbours))

    def halo_copy(kind, tile):
        src, dst, to, recv = (
            (kv_ref, hkv_ref, after, tile),
            (qg_ref, nqg_ref, before, TILES),
        )[kind]
        return pltpu.make_async_remote_copy(
            src_ref=src.at[tile],
            dst_ref=dst.at[tile],
            send_sem=halo_send.at[kind],
            recv_sem=halo_recv.at[recv],
            device_id=at_sp(to),
            device_id_type=MESH,
        )

    wait_bytes(kv_ref, load_sem.at[0])
    for tile in reversed(range(TILES)):
        halo_copy(0, tile).start()
    wait_bytes(qg_ref, load_sem.at[1])
    for tile in reversed(range(TILES)):
        halo_copy(1, tile).start()
    tell(level_1, axes)
    for load in small:
        load.wait()

    ones = (iota((LANES, LANES), 0) // HD == iota((LANES, LANES), 1) // HD).astype(bf16)
    qgain = jnp.concatenate([qgain_ref[...], qgain_ref[...]], axis=1)
    kgain = jnp.concatenate([kgain_ref[...], kgain_ref[...]], axis=1)

    key_i, query_i = iota((TILE, TILE), 0), iota((TILE, TILE), 1)
    reached = query_i >= key_i
    near, mid, far = [], [], []
    for h in range(2):
        row = bias_ref[h : h + 1, 0:LANES] * LOG2E
        last = bias_ref[h : h + 1, LANES : LANES + 1] * LOG2E
        table = shifted_rows(row)
        near.append(jnp.where(reached, table, OFF))
        mid.append(jnp.where(reached, last, table))
        far.append(jnp.broadcast_to(last, (1, TILE)))
    near = jnp.concatenate(near, axis=1)
    mid = jnp.concatenate(mid, axis=1)
    far = jnp.concatenate(far, axis=1)
    both_reached = jnp.concatenate([reached, reached], axis=1)
    wide_q = lax.rem(iota((TILE, WIDE), 1), TILE) // HD
    wide_k = iota((TILE, WIDE), 0) // HD
    edge = jnp.where(wide_k >= wide_q, 0.0, OFF)
    halo_off = jnp.where(sp > 0, 0.0, OFF)
    next_off = jnp.where(sp < nsp - 1, 0.0, OFF)

    def own_bias(distance):
        return (near, mid, far)[min(distance, 2)]

    def halo_bias(distance, off):
        if distance == 0:
            return far + edge + off
        return (mid if distance == TILES - 1 else far) + off

    for t in range(TILES):
        unit, scale, hat = normalize(qg_ref[t, 0:TILE], qgain, ones)
        unit_q[tiles[t]] = unit
        scale_q[tiles[t]] = scale
        qm_ref[wides[t]] = both_heads(hat)
        gm_ref[wides[t]] = both_heads(qg_ref[t, TILE:])
        unit, scale, hat = normalize(kv_ref[t, 0:TILE], kgain, ones)
        unit_k[tiles[t]] = unit
        scale_k[tiles[t]] = scale
        khat_ref[tiles[t]] = hat
        v_ref[tiles[t]] = kv_ref[t, TILE:]

    nt = ((1,), (1,))
    l_parts, n_parts = [], []
    for t in range(TILES):
        count = (t + 1) * TILE
        s = dot(khat_ref[0:count], qm_ref[wides[t]], nt)
        d = dot(v_ref[0:count], gm_ref[wides[t]], nt)
        l_sum = jnp.zeros((1, WIDE), f32)
        n_sum = jnp.zeros((1, WIDE), f32)
        for ck in range(t + 1):
            part = tiles[ck]
            slot = slice((TILES - t + ck) * TILE, (TILES - t + ck + 1) * TILE)
            e = jnp.exp2(s[part] * (SCALE * LOG2E) + own_bias(t - ck))
            e_ref[t, slot] = e
            d_ref[t, slot] = d[part]
            l_sum += jnp.sum(e, axis=0, keepdims=True)
            n_sum += jnp.sum(e * d[part], axis=0, keepdims=True)
        l_parts.append(l_sum)
        n_parts.append(n_sum)
    pl.semaphore_wait(level_1, len(axes))
    tell(level_2, two_away)

    def stat_copy(t):
        return pltpu.make_async_remote_copy(
            src_ref=send_stat.at[t],
            dst_ref=recv_stat.at[t],
            send_sem=stat_sem.at[0],
            recv_sem=stat_sem.at[1],
            device_id=at_sp(before),
            device_id_type=MESH,
        )

    total = jnp.zeros((1, WIDE), f32)
    near_sum = jnp.zeros((TILE, WIDE), f32)
    mid_sum = jnp.zeros((TILE, WIDE), f32)
    gain_sum = jnp.zeros((1, LANES), f32)
    for ck in reversed(range(TILES)):
        if ck == 1:
            pl.semaphore_wait(level_2, len(two_away))
            tell(level_3, four_away)
            tell(x_ready, x_peers)
        rows = tiles[ck]
        wait_bytes(hkv_ref.at[ck], halo_recv.at[ck])
        hkhat_ref[rows] = normalize(hkv_ref[ck, 0:TILE], kgain, ones)[2]
        span = (ck + 1) * WIDE
        s = dot(hkhat_ref[rows], qm_ref[0:span], nt)
        d = dot(hkv_ref[ck, TILE:], gm_ref[0:span], nt)
        for t in reversed(range(ck + 1)):
            part = wides[t]
            slot = slice((ck - t) * TILE, (ck - t + 1) * TILE)
            e = jnp.exp2(s[:, part] * (SCALE * LOG2E) + halo_bias(ck - t, halo_off))
            e_ref[t, slot] = e
            d_ref[t, slot] = d[:, part]
            l_parts[t] += jnp.sum(e, axis=0, keepdims=True)
            n_parts[t] += jnp.sum(e * d[:, part], axis=0, keepdims=True)
        t = ck
        inv = 1.0 / l_parts[t]
        delta = n_parts[t] * inv
        send_stat[t, 0:1] = inv
        send_stat[t, 1:2] = delta
        stat_copy(t).start()
        prob = e_ref[t] * inv
        grad = prob * (d_ref[t] - delta)
        total += jnp.sum(grad, axis=0, keepdims=True)
        own = (TILES - t) * TILE
        near_sum += grad[TILES * TILE :]
        mid_sum += grad[(TILES - 1) * TILE : TILES * TILE]
        low = grad.astype(bf16)
        low_ref[t] = low
        pown_ref[0 : (t + 1) * TILE, wides[t]] = prob[own:].astype(bf16)
        dk_t = dot(low, qm_ref[wides[t]])
        keys = jnp.concatenate([hkhat_ref[t * TILE :], khat_ref[0 : (t + 1) * TILE]], axis=0)
        gain_sum += jnp.sum(dk_t * keys.astype(f32), axis=0, keepdims=True)
        if t == TILES - 1:
            dk_acc[...] = dk_t[own:]
        else:
            dk_acc[0 : (t + 1) * TILE] += dk_t[own:]

    diagonals = jnp.where(both_reached, near_sum, mid_sum)
    taps = [diagonal_sums(diagonals[:, h * TILE : (h + 1) * TILE]) for h in range(2)]
    sums = [jnp.sum(total[:, h * TILE : (h + 1) * TILE], axis=1, keepdims=True) for h in range(2)]
    lane = iota((1, LANES), 1)
    sums = jnp.where(lane < HD, sums[0], sums[1])
    abuf[y] = jnp.concatenate([taps[0], taps[1], sums, gain_sum], axis=0)
    asend[...] = gain_sum

    a_offsets = [(dy, dx) for dx in range(nx) for dy in range(ny) if (dy, dx) != (0, 0)]

    def a_copy(dy, dx):
        to_y, to_x = lax.rem(y + dy, ny), lax.rem(x + dx, nx)
        kind = 0 if dx == 0 else 1
        return pltpu.make_async_remote_copy(
            src_ref=asend if kind else abuf.at[y],
            dst_ref=again.at[x * ny + y] if kind else abuf.at[y],
            send_sem=a_sem.at[kind],
            recv_sem=a_sem.at[2 + kind],
            device_id={"y": to_y, "x": to_x},
            device_id_type=MESH,
        )

    def wait_a(first):
        wait_bytes(abuf.at[pl.ds(0, ny - 1)], a_sem.at[first])
        if nx > 1:
            wait_bytes(again.at[pl.ds(0, ny * (nx - 1))], a_sem.at[first + 1])

    if x_peers:
        pl.semaphore_wait(x_ready, len(x_peers))
    for dy, dx in a_offsets:
        a_copy(dy, dx).start()

    wait_bytes(nqg_ref, halo_recv.at[TILES])
    for t in reversed(range(TILES)):
        qmn_ref[wides[t]] = both_heads(normalize(nqg_ref[t, 0:TILE], qgain, ones)[2])
        gmn_ref[wides[t]] = both_heads(nqg_ref[t, TILE:])
        s = dot(khat_ref[t * TILE :], qmn_ref[wides[t]], nt)
        d = dot(v_ref[t * TILE :], gmn_ref[wides[t]], nt)
        for ck in range(t, TILES):
            part = slice((ck - t) * TILE, (ck - t + 1) * TILE)
            en_ref[tiles[ck], wides[t]] = jnp.exp2(
                s[part] * (SCALE * LOG2E) + halo_bias(ck - t, next_off)
            )
            dn_ref[tiles[ck], wides[t]] = d[part]

    for t in range(TILES):
        rows = tiles[t]
        keys = jnp.concatenate([hkhat_ref[t * TILE :], khat_ref[0 : (t + 1) * TILE]], axis=0)
        dq_t = dot(keys, low_ref[t], ((0,), (0,)))
        dq_t = jnp.concatenate([dq_t[0:HD, 0:TILE], dq_t[HD:, TILE:]], axis=0) * SCALE
        dq_ref[rows] = norm_backward(
            dq_t.T, unit_q[rows], scale_q[rows], qgain, ones
        ).astype(bf16)

    pl.semaphore_wait(level_3, len(four_away))
    tell(c_ready, partner)
    wait_a(2)
    block = abuf[0]
    for i in range(1, ny):
        block += abuf[i]
    for i in range(ny):
        again[x * ny + i] = abuf[i, 3:4]
    gain_sum = again[0]
    for i in range(1, nx * ny):
        gain_sum += again[i]
    bbuf[z] = jnp.concatenate([block[0:3], gain_sum], axis=0)
    bsend[...] = gain_sum

    b_offsets = [(dz, dc) for dc in range(nc) for dz in range(nz) if (dz, dc) != (0, 0)]

    def b_copy(dz, dc):
        to_z, to_c = lax.rem(z + dz, nz), lax.rem(c + dc, nc)
        kind = 0 if dc == 0 else 1
        return pltpu.make_async_remote_copy(
            src_ref=bsend if kind else bbuf.at[z],
            dst_ref=bgain.at[c * nz + z] if kind else bbuf.at[z],
            send_sem=b_sem.at[kind],
            recv_sem=b_sem.at[2 + kind],
            device_id={"z": to_z, "c": to_c},
            device_id_type=MESH,
        )

    def wait_b(first):
        wait_bytes(bbuf.at[pl.ds(0, nz - 1)], b_sem.at[first])
        if nc > 1:
            wait_bytes(bgain.at[pl.ds(0, nz * (nc - 1))], b_sem.at[first + 1])

    if partner:
        pl.semaphore_wait(c_ready, len(partner))
    for dz, dc in b_offsets:
        b_copy(dz, dc).start()

    wait_bytes(recv_stat, stat_sem.at[1])
    for t in reversed(range(TILES)):
        inv, delta = recv_stat[t, 0:1], recv_stat[t, 1:2]
        prob = en_ref[t * TILE :, wides[t]] * inv
        pn_ref[t * TILE :, wides[t]] = prob.astype(bf16)
        sn_ref[t * TILE :, wides[t]] = (prob * (dn_ref[t * TILE :, wides[t]] - delta)).astype(bf16)

    for ck in range(TILES):
        rows = tiles[ck]
        own, later = slice(ck * WIDE, TILES * WIDE), slice(0, (ck + 1) * WIDE)
        dv = dot(pown_ref[rows, own], gm_ref[own]) + dot(pn_ref[rows, later], gmn_ref[later])
        dv_ref[rows] = dv.astype(bf16)
        dk = dk_acc[rows] + dot(sn_ref[rows, later], qmn_ref[later])
        dk_ref[rows] = norm_backward(
            dk * SCALE, unit_k[rows], scale_k[rows], kgain, ones
        ).astype(bf16)

    wait_bytes(kv_ref, halo_send.at[0])
    wait_bytes(qg_ref, halo_send.at[1])
    wait_bytes(send_stat, stat_sem.at[0])
    wait_a(0)

    wait_b(2)
    block = bbuf[0]
    for i in range(1, nz):
        block += bbuf[i]
    for i in range(nz):
        bgain[c * nz + i] = bbuf[i, 3:4]
    gain_sum = bgain[0]
    for i in range(1, nc * nz):
        gain_sum += bgain[i]
    for h in range(2):
        taps = block[h : h + 1]
        rest = block[2:3, h * HD : h * HD + 1] - jnp.sum(taps, axis=1, keepdims=True)
        dbias_ref[h : h + 1, 0:LANES] = taps
        dbias_ref[h : h + 1, LANES : LANES + 1] = rest
    gain_sum = (gain_sum + pltpu.roll(gain_sum, HD, 1))[:, 0:HD] * SCALE
    dqgain_ref[...] = gain_sum / qgain_ref[...]
    dkgain_ref[...] = gain_sum / kgain_ref[...]
    wait_b(0)


def flush(*refs):
    count = len(refs) // 2
    sems = refs[-1]
    copies = [
        pltpu.make_async_copy(refs[i], refs[count + i], sems.at[i]) for i in range(count)
    ]
    for copy in copies:
        copy.start()
    for copy in copies:
        copy.wait()


def per_device(sizes, query, key, value, out_grad, query_gain, key_gain, rel_bias):
    nz, ny, nx, nc = sizes
    vmem = pl.BlockSpec(memory_space=pltpu.VMEM)
    hbm = pl.BlockSpec(memory_space=pl.ANY)
    dma = pltpu.SemaphoreType.DMA
    regular = pltpu.SemaphoreType.REGULAR
    shapes = (((ROWS, LANES), bf16),) * 3 + (((1, HD), f32),) * 2 + ((rel_bias.shape, f32),)
    tile_rows, wide_rows = (ROWS, LANES), (TILES * WIDE, LANES)
    square = (ROWS, TILES * WIDE)
    outs = pl.pallas_call(
        functools.partial(body, sizes),
        out_shape=tuple(pltpu.VMEM(*s) for s in shapes),
        in_specs=[hbm] * 7,
        out_specs=(vmem,) * 6,
        scratch_shapes=[
            *[pltpu.VMEM((1, HD), f32)] * 2,
            pltpu.VMEM(rel_bias.shape, f32),
            *[pltpu.VMEM((TILES, 2 * TILE, LANES), bf16)] * 4,
            *[pltpu.VMEM((TILES, 2, WIDE), f32)] * 2,
            *[pltpu.VMEM(tile_rows, f32)] * 5,
            *[pltpu.VMEM(tile_rows, bf16)] * 3,
            *[pltpu.VMEM(wide_rows, bf16)] * 4,
            *[pltpu.VMEM((TILES, (TILES + 1) * TILE, WIDE), f32)] * 2,
            pltpu.VMEM((TILES, (TILES + 1) * TILE, WIDE), bf16),
            *[pltpu.VMEM(square, f32)] * 2,
            *[pltpu.VMEM(square, bf16)] * 3,
            pltpu.VMEM((ny, 4, LANES), f32),
            pltpu.VMEM((nx * ny, 1, LANES), f32),
            pltpu.VMEM((1, LANES), f32),
            pltpu.VMEM((nz, 4, LANES), f32),
            pltpu.VMEM((nc * nz, 1, LANES), f32),
            pltpu.VMEM((1, LANES), f32),
            dma((5,)),
            dma((TILES + 1,)),
            dma((2,)),
            dma((2,)),
            dma((4,)),
            dma((4,)),
            regular((5,)),
        ],
        compiler_params=pltpu.CompilerParams(collective_id=0, has_side_effects=True),
        name="segment_backward",
    )(query, key, value, out_grad, query_gain.reshape(1, HD), key_gain.reshape(1, HD), rel_bias)
    outs = pl.pallas_call(
        flush,
        out_shape=tuple(jax.ShapeDtypeStruct(*s) for s in shapes),
        in_specs=[vmem] * 6,
        out_specs=(hbm,) * 6,
        scratch_shapes=[dma((6,))],
        name="flush",
    )(*(pltpu.with_memory_space_constraint(o, pltpu.VMEM) for o in outs))
    return (*outs[:3], outs[3].reshape(HD), outs[4].reshape(HD), outs[5])


def solution(mesh):
    sizes = mesh_sizes(mesh)
    torus = Mesh(mesh.devices.reshape(sizes), ("z", "y", "x", "c"))
    return jax.shard_map(
        functools.partial(per_device, sizes),
        mesh=torus,
        in_specs=(P(SP, TP), P(SP, TP), P(SP, TP), P(SP, TP), P(), P(), P(TP, None)),
        out_specs=(P(SP, TP), P(SP, TP), P(SP, TP), P(), P(), P(TP, None)),
        check_vma=False,
    )


def mesh_sizes(mesh):
    return (16, 8, 4, 2)
```

time: 45.2 us -> 43.7 us (0.967)
  Pallas kernels: 44.5 us -> 42.8 us
    pallas_call x1, Pallas kernels: 43.7 us -> 42 us  [per_device(): pl.pallas_call(functools.partial(body, sizes), out_shape=tuple((pltpu.VME...]
where the time goes in v3:
time: 43.7 us; the launch traced here: 43.5 us
  Pallas kernels  42.8 us (98%)
  between operations  0.64 us (1%)
    pallas_call x1, Pallas kernels, per_device(): pl.pallas_call(functools.partial(body, sizes), out_shape=tuple((pltpu.VME...  42 us

profile of v3, /device:TPU:1, one launch (start us, length us, event | category | flops | bytes accessed | tf_op | source)
XLA Modules:
  0.0 43.5 jit_solution(7731900502148320995)
XLA Ops:
  0.6 42.0 %segment_backward.1 = (bf16[512,128]{1,0:T(8,128)(2,1)S(1)}, bf16[512,128]{1,0:T(8,128)(2,1)S(1)}, bf16[512,128]{1,0:T(8,128)(2,1)S(1)}, f32[1,64]{1,0:T(1,128)S...) custom-call(bf16[512,128]{1,0:T(8,128)(2,1)} %q_hbm.1, bf16[512,128]{1,0:T(8,128)(2,1)} %k_hbm.1, bf16[512,128]{1,0:T(8,128)(2,1)} %v_hbm.1, ...), custom_call_target="tpu_custom_call" | custom-call | tf_op jit(solution)/shard_map/segment_backward/pallas_call | solution.py:491
  42.7 0.8 %flush.1 = (bf16[512,128]{1,0:T(8,128)(2,1)}, bf16[512,128]{1,0:T(8,128)(2,1)}, bf16[512,128]{1,0:T(8,128)(2,1)}, f32[1,64]{1,0:T(1,128)}, f32[1,64]{1,0:T(1,128)}, /*index=5*/f32[2,129]{1,0:T(2,128)}) custom-call(bf16[512,128]{1,0:T(8,128)(2,1)S(1)} %get-tuple-element.18.refs_0_, bf16[512,128]{1,0:T(8,128)(2,1)S(1)} %get-tuple-element.19.refs_1_, ...), custom_call_target="tpu_custom_call" | custom-call | tf_op jit(solution)/shard_map/flush/pallas_call | solution.py:525

commit v4 on v3

--- a/solution.py
+++ b/solution.py
@@ -108,7 +108,7 @@
     scale_k,
     dk_acc,
     khat_ref,
-    hkhat_ref,
+    k_ref,
     v_ref,
     qm_ref,
     gm_ref,
@@ -125,15 +125,17 @@
     abuf,
     again,
     asend,
+    gain_yx,
     bbuf,
-    bgain,
-    bsend,
+    cbuf,
+    zgain,
     load_sem,
     halo_recv,
     halo_send,
     stat_sem,
     a_sem,
     b_sem,
+    c_sem,
     level,
 ):
     nz, ny, nx, nc = sizes
@@ -158,6 +160,8 @@
     def wait_bytes(ref, sem):
         pltpu.make_async_copy(ref, ref, sem).wait()
 
+    lead = nc - 1
+    at_lead = c == lead
     axes = both_ways("z", z, nz, 1) + both_ways("y", y, ny, 1)
     if nx > 1:
         axes += both_ways("x", x, nx, 1)
@@ -165,7 +169,7 @@
     x_peers = [{"x": lax.rem(x + d, nx)} for d in range(1, nx)]
     two_away = both_ways("z", z, nz, 2) + both_ways("y", y, ny, 2)
     four_away = both_ways("z", z, nz, 4)
-    level_1, level_2, level_3, x_ready, c_ready = (level.at[i] for i in range(5))
+    level_1, level_2, level_3, x_ready, c_ready, z_ready = (level.at[i] for i in range(6))
 
     barrier = pltpu.get_barrier_semaphore()
     neighbours = [at_sp(after), at_sp(before)] + axes + partner
@@ -173,19 +177,34 @@
 
     tiles = [slice(t * TILE, (t + 1) * TILE) for t in range(TILES)]
     wides = [slice(t * WIDE, (t + 1) * WIDE) for t in range(TILES)]
-    for first, second, ref, sem in ((k_hbm, v_hbm, kv_ref, 0), (q_hbm, g_hbm, qg_ref, 1)):
-        for t in reversed(range(TILES)):
-            for half, src in enumerate((first, second)):
-                dst = ref.at[t, pl.ds(half * TILE, TILE)]
-                pltpu.make_async_copy(src.at[tiles[t]], dst, load_sem.at[sem]).start()
     small = [
-        pltpu.make_async_copy(src, dst, load_sem.at[2 + i])
+        pltpu.make_async_copy(src, dst, load_sem.at[3 + i])
         for i, (src, dst) in enumerate(
-            ((qgain_hbm, qgain_ref), (kgain_hbm, kgain_ref), (bias_hbm, bias_ref))
+            ((kgain_hbm, kgain_ref), (qgain_hbm, qgain_ref), (bias_hbm, bias_ref))
         )
     ]
+    load_keys = pltpu.make_async_copy(k_hbm, k_ref, load_sem.at[0])
+    load_keys.start()
     for load in small:
         load.start()
+    for t in reversed(range(TILES)):
+        dst = kv_ref.at[t, pl.ds(TILE, TILE)]
+        pltpu.make_async_copy(v_hbm.at[tiles[t]], dst, load_sem.at[1]).start()
+    for t in reversed(range(TILES)):
+        for half, src in enumerate((q_hbm, g_hbm)):
+            dst = qg_ref.at[t, pl.ds(half * TILE, TILE)]
+            pltpu.make_async_copy(src.at[tiles[t]], dst, load_sem.at[2]).start()
+
+    ones = (iota((LANES, LANES), 0) // HD == iota((LANES, LANES), 1) // HD).astype(bf16)
+    small[0].wait()
+    kgain = jnp.concatenate([kgain_ref[...], kgain_ref[...]], axis=1)
+    load_keys.wait()
+    for t in reversed(range(TILES)):
+        unit, scale, hat = normalize(k_ref[tiles[t]], kgain, ones)
+        unit_k[tiles[t]] = unit
+        scale_k[tiles[t]] = scale
+        khat_ref[tiles[t]] = hat
+        kv_ref[t, 0:TILE] = hat
     pl.semaphore_wait(barrier, len(neighbours))
 
     def halo_copy(kind, tile):
@@ -202,19 +221,17 @@
             device_id_type=MESH,
         )
 
-    wait_bytes(kv_ref, load_sem.at[0])
+    wait_bytes(v_ref, load_sem.at[1])
     for tile in reversed(range(TILES)):
         halo_copy(0, tile).start()
-    wait_bytes(qg_ref, load_sem.at[1])
+    wait_bytes(qg_ref, load_sem.at[2])
     for tile in reversed(range(TILES)):
         halo_copy(1, tile).start()
     tell(level_1, axes)
-    for load in small:
+    for load in small[1:]:
         load.wait()
 
-    ones = (iota((LANES, LANES), 0) // HD == iota((LANES, LANES), 1) // HD).astype(bf16)
     qgain = jnp.concatenate([qgain_ref[...], qgain_ref[...]], axis=1)
-    kgain = jnp.concatenate([kgain_ref[...], kgain_ref[...]], axis=1)
 
     key_i, query_i = iota((TILE, TILE), 0), iota((TILE, TILE), 1)
     reached = query_i >= key_i
@@ -250,10 +267,6 @@
         scale_q[tiles[t]] = scale
         qm_ref[wides[t]] = both_heads(hat)
         gm_ref[wides[t]] = both_heads(qg_ref[t, TILE:])
-        unit, scale, hat = normalize(kv_ref[t, 0:TILE], kgain, ones)
-        unit_k[tiles[t]] = unit
-        scale_k[tiles[t]] = scale
-        khat_ref[tiles[t]] = hat
         v_ref[tiles[t]] = kv_ref[t, TILE:]
 
     nt = ((1,), (1,))
@@ -287,20 +300,30 @@
             device_id_type=MESH,
         )
 
+    def keys_of(t):
+        halo = [hkv_ref[ck, 0:TILE] for ck in range(t, TILES)]
+        return jnp.concatenate(halo + [khat_ref[0 : (t + 1) * TILE]], axis=0)
+
     total = jnp.zeros((1, WIDE), f32)
     near_sum = jnp.zeros((TILE, WIDE), f32)
     mid_sum = jnp.zeros((TILE, WIDE), f32)
     gain_sum = jnp.zeros((1, LANES), f32)
     for ck in reversed(range(TILES)):
-        if ck == 1:
+        if ck == TILES - 2:
             pl.semaphore_wait(level_2, len(two_away))
             tell(level_3, four_away)
             tell(x_ready, x_peers)
-        rows = tiles[ck]
         wait_bytes(hkv_ref.at[ck], halo_recv.at[ck])
-        hkhat_ref[rows] = normalize(hkv_ref[ck, 0:TILE], kgain, ones)[2]
+        if ck == 0:
+            if x_peers:
+                pl.semaphore_wait(x_ready, len(x_peers))
+
+            @pl.when(at_lead)
+            def _():
+                tell(c_ready, partner)
+
         span = (ck + 1) * WIDE
-        s = dot(hkhat_ref[rows], qm_ref[0:span], nt)
+        s = dot(hkv_ref[ck, 0:TILE], qm_ref[0:span], nt)
         d = dot(hkv_ref[ck, TILE:], gm_ref[0:span], nt)
         for t in reversed(range(ck + 1)):
             part = wides[t]
@@ -315,7 +338,6 @@
         delta = n_parts[t] * inv
         send_stat[t, 0:1] = inv
         send_stat[t, 1:2] = delta
-        stat_copy(t).start()
         prob = e_ref[t] * inv
         grad = prob * (d_ref[t] - delta)
         total += jnp.sum(grad, axis=0, keepdims=True)
@@ -326,7 +348,7 @@
         low_ref[t] = low
         pown_ref[0 : (t + 1) * TILE, wides[t]] = prob[own:].astype(bf16)
         dk_t = dot(low, qm_ref[wides[t]])
-        keys = jnp.concatenate([hkhat_ref[t * TILE :], khat_ref[0 : (t + 1) * TILE]], axis=0)
+        keys = keys_of(t)
         gain_sum += jnp.sum(dk_t * keys.astype(f32), axis=0, keepdims=True)
         if t == TILES - 1:
             dk_acc[...] = dk_t[own:]
@@ -335,35 +357,54 @@
 
     diagonals = jnp.where(both_reached, near_sum, mid_sum)
     taps = [diagonal_sums(diagonals[:, h * TILE : (h + 1) * TILE]) for h in range(2)]
-    sums = [jnp.sum(total[:, h * TILE : (h + 1) * TILE], axis=1, keepdims=True) for h in range(2)]
-    lane = iota((1, LANES), 1)
-    sums = jnp.where(lane < HD, sums[0], sums[1])
+    folded = [total[:, h * TILE : (h + 1) * TILE] for h in range(2)]
+    folded = [part + pltpu.roll(part, HD, 1) for part in folded]
+    first_half = iota((1, LANES), 1) < HD
+    sums = jnp.where(first_half, folded[0], folded[1])
+    asend[...] = gain_sum
     abuf[y] = jnp.concatenate([taps[0], taps[1], sums, gain_sum], axis=0)
-    asend[...] = gain_sum
-
-    a_offsets = [(dy, dx) for dx in range(nx) for dy in range(ny) if (dy, dx) != (0, 0)]
-
-    def a_copy(dy, dx):
-        to_y, to_x = lax.rem(y + dy, ny), lax.rem(x + dx, nx)
-        kind = 0 if dx == 0 else 1
+
+    group = ny * nx
+    others = [(dy, dx) for dx in range(nx) for dy in range(ny)][1:]
+    others.sort(key=lambda o: -min(o[0], ny - o[0]) - min(o[1], nx - o[1]))
+    y_others = sorted(range(1, ny), key=lambda d: -min(d, ny - d))
+    z_others = sorted(range(1, nz), key=lambda d: -min(d, nz - d))
+
+    def gain_copy(dy, dx):
         return pltpu.make_async_remote_copy(
-            src_ref=asend if kind else abuf.at[y],
-            dst_ref=again.at[x * ny + y] if kind else abuf.at[y],
-            send_sem=a_sem.at[kind],
-            recv_sem=a_sem.at[2 + kind],
-            device_id={"y": to_y, "x": to_x},
+            src_ref=asend,
+            dst_ref=again.at[c * group + x * ny + y],
+            send_sem=a_sem.at[1],
+            recv_sem=a_sem.at[3],
+            device_id={"y": lax.rem(y + dy, ny), "x": lax.rem(x + dx, nx), "c": lead},
             device_id_type=MESH,
         )
 
-    def wait_a(first):
-        wait_bytes(abuf.at[pl.ds(0, ny - 1)], a_sem.at[first])
-        if nx > 1:
-            wait_bytes(again.at[pl.ds(0, ny * (nx - 1))], a_sem.at[first + 1])
-
-    if x_peers:
-        pl.semaphore_wait(x_ready, len(x_peers))
-    for dy, dx in a_offsets:
-        a_copy(dy, dx).start()
+    def a_copy(dy):
+        return pltpu.make_async_remote_copy(
+            src_ref=abuf.at[y],
+            dst_ref=abuf.at[y],
+            send_sem=a_sem.at[0],
+            recv_sem=a_sem.at[2],
+            device_id={"y": lax.rem(y + dy, ny)},
+            device_id_type=MESH,
+        )
+
+    @pl.when(jnp.logical_not(at_lead))
+    def _():
+        pl.semaphore_wait(c_ready, 1)
+
+    for dy, dx in others:
+        gain_copy(dy, dx).start()
+
+    @pl.when(jnp.logical_not(at_lead))
+    def _():
+        gain_copy(0, 0).start()
+
+    for dy in y_others:
+        a_copy(dy).start()
+    for t in range(TILES):
+        stat_copy(t).start()
 
     wait_bytes(nqg_ref, halo_recv.at[TILES])
     for t in reversed(range(TILES)):
@@ -378,52 +419,68 @@
             )
             dn_ref[tiles[ck], wides[t]] = d[part]
 
+    pl.semaphore_wait(level_3, len(four_away))
+
+    @pl.when(jnp.logical_not(at_lead))
+    def _():
+        tell(z_ready, [{"c": lead}])
+
     for t in range(TILES):
         rows = tiles[t]
-        keys = jnp.concatenate([hkhat_ref[t * TILE :], khat_ref[0 : (t + 1) * TILE]], axis=0)
+        keys = keys_of(t)
         dq_t = dot(keys, low_ref[t], ((0,), (0,)))
         dq_t = jnp.concatenate([dq_t[0:HD, 0:TILE], dq_t[HD:, TILE:]], axis=0) * SCALE
         dq_ref[rows] = norm_backward(
             dq_t.T, unit_q[rows], scale_q[rows], qgain, ones
         ).astype(bf16)
 
-    pl.semaphore_wait(level_3, len(four_away))
-    tell(c_ready, partner)
-    wait_a(2)
+    @pl.when(at_lead)
+    def _():
+        wait_bytes(again.at[pl.ds(0, nc * group - 1)], a_sem.at[3])
+        again[c * group + x * ny + y] = asend[...]
+        gains = again[0]
+        for i in range(1, nc * group):
+            gains += again[i]
+        gain_yx[...] = gains
+
+    wait_bytes(abuf.at[pl.ds(0, ny - 1)], a_sem.at[2])
     block = abuf[0]
     for i in range(1, ny):
         block += abuf[i]
-    for i in range(ny):
-        again[x * ny + i] = abuf[i, 3:4]
-    gain_sum = again[0]
-    for i in range(1, nx * ny):
-        gain_sum += again[i]
-    bbuf[z] = jnp.concatenate([block[0:3], gain_sum], axis=0)
-    bsend[...] = gain_sum
-
-    b_offsets = [(dz, dc) for dc in range(nc) for dz in range(nz) if (dz, dc) != (0, 0)]
-
-    def b_copy(dz, dc):
-        to_z, to_c = lax.rem(z + dz, nz), lax.rem(c + dc, nc)
-        kind = 0 if dc == 0 else 1
+    bbuf[z] = block
+
+    @pl.when(at_lead)
+    def _():
+        bbuf[z, 3:4] = gain_yx[...]
+
+    def b_copy(dz):
         return pltpu.make_async_remote_copy(
-            src_ref=bsend if kind else bbuf.at[z],
-            dst_ref=bgain.at[c * nz + z] if kind else bbuf.at[z],
-            send_sem=b_sem.at[kind],
-            recv_sem=b_sem.at[2 + kind],
-            device_id={"z": to_z, "c": to_c},
+            src_ref=bbuf.at[z],
+            dst_ref=bbuf.at[z],
+            send_sem=b_sem.at[0],
+            recv_sem=b_sem.at[1],
+            device_id={"z": lax.rem(z + dz, nz)},
             device_id_type=MESH,
         )
 
-    def wait_b(first):
-        wait_bytes(bbuf.at[pl.ds(0, nz - 1)], b_sem.at[first])
-        if nc > 1:
-            wait_bytes(bgain.at[pl.ds(0, nz * (nc - 1))], b_sem.at[first + 1])
-
-    if partner:
-        pl.semaphore_wait(c_ready, len(partner))
-    for dz, dc in b_offsets:
-        b_copy(dz, dc).start()
+    def down_copy(dz):
+        return pltpu.make_async_remote_copy(
+            src_ref=gain_yx,
+            dst_ref=zgain.at[z],
+            send_sem=c_sem.at[0],
+            recv_sem=c_sem.at[1],
+            device_id={"z": lax.rem(z + dz, nz), "c": 0},
+            device_id_type=MESH,
+        )
+
+    for dz in z_others:
+        b_copy(dz).start()
+
+    @pl.when(at_lead)
+    def _():
+        pl.semaphore_wait(z_ready, 1)
+        for dz in z_others + [0]:
+            down_copy(dz).start()
 
     wait_bytes(recv_stat, stat_sem.at[1])
     for t in reversed(range(TILES)):
@@ -445,26 +502,48 @@
     wait_bytes(kv_ref, halo_send.at[0])
     wait_bytes(qg_ref, halo_send.at[1])
     wait_bytes(send_stat, stat_sem.at[0])
-    wait_a(0)
-
-    wait_b(2)
+    wait_bytes(abuf.at[pl.ds(0, ny - 1)], a_sem.at[0])
+
+    @pl.when(at_lead)
+    def _():
+        wait_bytes(again.at[pl.ds(0, group - 1)], a_sem.at[1])
+
+    @pl.when(jnp.logical_not(at_lead))
+    def _():
+        wait_bytes(again.at[pl.ds(0, group)], a_sem.at[1])
+
+    wait_bytes(bbuf.at[pl.ds(0, nz - 1)], b_sem.at[1])
     block = bbuf[0]
     for i in range(1, nz):
         block += bbuf[i]
-    for i in range(nz):
-        bgain[c * nz + i] = bbuf[i, 3:4]
-    gain_sum = bgain[0]
-    for i in range(1, nc * nz):
-        gain_sum += bgain[i]
+
+    @pl.when(at_lead)
+    def _():
+        cbuf[...] = block[3:4]
+
+    @pl.when(jnp.logical_not(at_lead))
+    def _():
+        wait_bytes(zgain, c_sem.at[1])
+        gains = zgain[0]
+        for i in range(1, nz):
+            gains += zgain[i]
+        cbuf[...] = gains
+
     for h in range(2):
         taps = block[h : h + 1]
-        rest = block[2:3, h * HD : h * HD + 1] - jnp.sum(taps, axis=1, keepdims=True)
+        rest = jnp.where(first_half if h == 0 else ~first_half, block[2:3], 0.0) - taps
         dbias_ref[h : h + 1, 0:LANES] = taps
-        dbias_ref[h : h + 1, LANES : LANES + 1] = rest
+        dbias_ref[h : h + 1, LANES : LANES + 1] = jnp.sum(rest, axis=1, keepdims=True)
+
+    gain_sum = cbuf[...]
     gain_sum = (gain_sum + pltpu.roll(gain_sum, HD, 1))[:, 0:HD] * SCALE
     dqgain_ref[...] = gain_sum / qgain_ref[...]
     dkgain_ref[...] = gain_sum / kgain_ref[...]
-    wait_b(0)
+    wait_bytes(bbuf.at[pl.ds(0, nz - 1)], b_sem.at[0])
+
+    @pl.when(at_lead)
+    def _():
+        wait_bytes(zgain, c_sem.at[0])
 
 
 def flush(*refs):
@@ -506,18 +585,20 @@
             *[pltpu.VMEM(square, f32)] * 2,
             *[pltpu.VMEM(square, bf16)] * 3,
             pltpu.VMEM((ny, 4, LANES), f32),
-            pltpu.VMEM((nx * ny, 1, LANES), f32),
+            pltpu.VMEM((nc * nx * ny, 1, LANES), f32),
+            pltpu.VMEM((1, LANES), f32),
             pltpu.VMEM((1, LANES), f32),
             pltpu.VMEM((nz, 4, LANES), f32),
-            pltpu.VMEM((nc * nz, 1, LANES), f32),
             pltpu.VMEM((1, LANES), f32),
-            dma((5,)),
+            pltpu.VMEM((nz, 1, LANES), f32),
+            dma((6,)),
             dma((TILES + 1,)),
             dma((2,)),
             dma((2,)),
             dma((4,)),
-            dma((4,)),
-            regular((5,)),
+            dma((2,)),
+            dma((2,)),
+            regular((6,)),
         ],
         compiler_params=pltpu.CompilerParams(collective_id=0, has_side_effects=True),
         name="segment_backward",

time: 43.7 us -> 42.5 us (0.973)
  Pallas kernels: 42.8 us -> 41.7 us
    pallas_call x1, Pallas kernels: 42 us -> 40.9 us  [per_device(): pl.pallas_call(functools.partial(body, sizes), out_shape=tuple((pltpu.VME...]
where the time goes in v4:
time: 42.5 us; the launch traced here: 42.3 us
  Pallas kernels  41.7 us (98%)
  between operations  0.64 us (2%)
    pallas_call x1, Pallas kernels, per_device(): pl.pallas_call(functools.partial(body, sizes), out_shape=tuple((pltpu.VME...  40.9 us

profile of v4, /device:TPU:1, one launch (start us, length us, event | category | flops | bytes accessed | tf_op | source)
XLA Modules:
  0.0 42.3 jit_solution(6188399134174977078)
XLA Ops:
  0.6 40.9 %segment_backward.1 = (bf16[512,128]{1,0:T(8,128)(2,1)S(1)}, bf16[512,128]{1,0:T(8,128)(2,1)S(1)}, bf16[512,128]{1,0:T(8,128)(2,1)S(1)}, f32[1,64]{1,0:T(1,128)S...) custom-call(bf16[512,128]{1,0:T(8,128)(2,1)} %q_hbm.1, bf16[512,128]{1,0:T(8,128)(2,1)} %k_hbm.1, bf16[512,128]{1,0:T(8,128)(2,1)} %v_hbm.1, ...), custom_call_target="tpu_custom_call" | custom-call | tf_op jit(solution)/shard_map/segment_backward/pallas_call | solution.py:570
  41.5 0.8 %flush.1 = (bf16[512,128]{1,0:T(8,128)(2,1)}, bf16[512,128]{1,0:T(8,128)(2,1)}, bf16[512,128]{1,0:T(8,128)(2,1)}, f32[1,64]{1,0:T(1,128)}, f32[1,64]{1,0:T(1,128)}, /*index=5*/f32[2,129]{1,0:T(2,128)}) custom-call(bf16[512,128]{1,0:T(8,128)(2,1)S(1)} %get-tuple-element.18.refs_0_, bf16[512,128]{1,0:T(8,128)(2,1)S(1)} %get-tuple-element.19.refs_1_, ...), custom_call_target="tpu_custom_call" | custom-call | tf_op jit(solution)/shard_map/flush/pallas_call | solution.py:606

commit v5 on v4

--- a/solution.py
+++ b/solution.py
@@ -70,6 +70,13 @@
     for bit in (1, 2, 4):
         block = jnp.where((index & bit) != 0, pltpu.roll(block, LANES - bit, 1), block)
     return jnp.sum(block, axis=0, keepdims=True)
+
+
+def tree_sum(parts):
+    while len(parts) > 1:
+        odd = parts[len(parts) // 2 * 2 :]
+        parts = [parts[i] + parts[i + 1] for i in range(0, len(parts) - 1, 2)] + odd
+    return parts[0]
 
 
 def both_heads(a):
@@ -169,10 +176,12 @@
     x_peers = [{"x": lax.rem(x + d, nx)} for d in range(1, nx)]
     two_away = both_ways("z", z, nz, 2) + both_ways("y", y, ny, 2)
     four_away = both_ways("z", z, nz, 4)
-    level_1, level_2, level_3, x_ready, c_ready, z_ready = (level.at[i] for i in range(6))
+    level_1, level_2, level_3, x_ready, c_ready, z_ready, link_free = (
+        level.at[i] for i in range(7)
+    )
 
     barrier = pltpu.get_barrier_semaphore()
-    neighbours = [at_sp(after), at_sp(before)] + axes + partner
+    neighbours = [at_sp(before), at_sp(after)] + axes + partner
     tell(barrier, neighbours)
 
     tiles = [slice(t * TILE, (t + 1) * TILE) for t in range(TILES)]
@@ -215,15 +224,20 @@
         return pltpu.make_async_remote_copy(
             src_ref=src.at[tile],
             dst_ref=dst.at[tile],
-            send_sem=halo_send.at[kind],
+            send_sem=halo_send.at[2 if kind == 0 and tile < TILES - 1 else kind],
             recv_sem=halo_recv.at[recv],
             device_id=at_sp(to),
             device_id_type=MESH,
         )
 
     wait_bytes(v_ref, load_sem.at[1])
-    for tile in reversed(range(TILES)):
-        halo_copy(0, tile).start()
+    halo_copy(0, TILES - 1).start()
+
+    @pl.when(jnp.logical_not(at_lead))
+    def _():
+        for tile in reversed(range(TILES - 1)):
+            halo_copy(0, tile).start()
+
     wait_bytes(qg_ref, load_sem.at[2])
     for tile in reversed(range(TILES)):
         halo_copy(1, tile).start()
@@ -290,6 +304,17 @@
     pl.semaphore_wait(level_1, len(axes))
     tell(level_2, two_away)
 
+    @pl.when(jnp.logical_not(at_lead))
+    def _():
+        wait_bytes(kv_ref.at[TILES - 1], halo_send.at[0])
+        tell(link_free, [{"c": lead}])
+
+    @pl.when(at_lead)
+    def _():
+        pl.semaphore_wait(link_free, 1)
+        for tile in reversed(range(TILES - 1)):
+            halo_copy(0, tile).start()
+
     def stat_copy(t):
         return pltpu.make_async_remote_copy(
             src_ref=send_stat.at[t],
@@ -304,24 +329,34 @@
         halo = [hkv_ref[ck, 0:TILE] for ck in range(t, TILES)]
         return jnp.concatenate(halo + [khat_ref[0 : (t + 1) * TILE]], axis=0)
 
+    def key_side(t):
+        own = (TILES - t) * TILE
+        dk_t = dot(low_ref[t], qm_ref[wides[t]])
+        if t == TILES - 1:
+            dk_acc[...] = dk_t[own:]
+        else:
+            dk_acc[0 : (t + 1) * TILE] += dk_t[own:]
+        return jnp.sum(dk_t * keys_of(t).astype(f32), axis=0, keepdims=True)
+
     total = jnp.zeros((1, WIDE), f32)
     near_sum = jnp.zeros((TILE, WIDE), f32)
     mid_sum = jnp.zeros((TILE, WIDE), f32)
     gain_sum = jnp.zeros((1, LANES), f32)
     for ck in reversed(range(TILES)):
-        if ck == TILES - 2:
+        wait_bytes(hkv_ref.at[ck], halo_recv.at[ck])
+        if ck == TILES - 1:
             pl.semaphore_wait(level_2, len(two_away))
             tell(level_3, four_away)
             tell(x_ready, x_peers)
-        wait_bytes(hkv_ref.at[ck], halo_recv.at[ck])
         if ck == 0:
-            if x_peers:
-                pl.semaphore_wait(x_ready, len(x_peers))
 
             @pl.when(at_lead)
             def _():
+                pl.semaphore_wait(x_ready, len(x_peers))
                 tell(c_ready, partner)
 
+        if ck < TILES - 1:
+            gain_sum += key_side(ck + 1)
         span = (ck + 1) * WIDE
         s = dot(hkv_ref[ck, 0:TILE], qm_ref[0:span], nt)
         d = dot(hkv_ref[ck, TILE:], gm_ref[0:span], nt)
@@ -346,14 +381,8 @@
         mid_sum += grad[(TILES - 1) * TILE : TILES * TILE]
         low = grad.astype(bf16)
         low_ref[t] = low
-        pown_ref[0 : (t + 1) * TILE, wides[t]] = prob[own:].astype(bf16)
-        dk_t = dot(low, qm_ref[wides[t]])
-        keys = keys_of(t)
-        gain_sum += jnp.sum(dk_t * keys.astype(f32), axis=0, keepdims=True)
-        if t == TILES - 1:
-            dk_acc[...] = dk_t[own:]
-        else:
-            dk_acc[0 : (t + 1) * TILE] += dk_t[own:]
+
+    gain_sum += key_side(0)
 
     diagonals = jnp.where(both_reached, near_sum, mid_sum)
     taps = [diagonal_sums(diagonals[:, h * TILE : (h + 1) * TILE]) for h in range(2)]
@@ -392,6 +421,7 @@
 
     @pl.when(jnp.logical_not(at_lead))
     def _():
+        pl.semaphore_wait(x_ready, len(x_peers))
         pl.semaphore_wait(c_ready, 1)
 
     for dy, dx in others:
@@ -427,6 +457,9 @@
 
     for t in range(TILES):
         rows = tiles[t]
+        own = (TILES - t) * TILE
+        prob = e_ref[t, own:] * send_stat[t, 0:1]
+        pown_ref[0 : (t + 1) * TILE, wides[t]] = prob.astype(bf16)
         keys = keys_of(t)
         dq_t = dot(keys, low_ref[t], ((0,), (0,)))
         dq_t = jnp.concatenate([dq_t[0:HD, 0:TILE], dq_t[HD:, TILE:]], axis=0) * SCALE
@@ -438,15 +471,10 @@
     def _():
         wait_bytes(again.at[pl.ds(0, nc * group - 1)], a_sem.at[3])
         again[c * group + x * ny + y] = asend[...]
-        gains = again[0]
-        for i in range(1, nc * group):
-            gains += again[i]
-        gain_yx[...] = gains
+        gain_yx[...] = tree_sum([again[i] for i in range(nc * group)])
 
     wait_bytes(abuf.at[pl.ds(0, ny - 1)], a_sem.at[2])
-    block = abuf[0]
-    for i in range(1, ny):
-        block += abuf[i]
+    block = tree_sum([abuf[i] for i in range(ny)])
     bbuf[z] = block
 
     @pl.when(at_lead)
@@ -499,13 +527,14 @@
             dk * SCALE, unit_k[rows], scale_k[rows], kgain, ones
         ).astype(bf16)
 
-    wait_bytes(kv_ref, halo_send.at[0])
     wait_bytes(qg_ref, halo_send.at[1])
+    wait_bytes(kv_ref.at[pl.ds(0, TILES - 1)], halo_send.at[2])
     wait_bytes(send_stat, stat_sem.at[0])
     wait_bytes(abuf.at[pl.ds(0, ny - 1)], a_sem.at[0])
 
     @pl.when(at_lead)
     def _():
+        wait_bytes(kv_ref.at[TILES - 1], halo_send.at[0])
         wait_bytes(again.at[pl.ds(0, group - 1)], a_sem.at[1])
 
     @pl.when(jnp.logical_not(at_lead))
@@ -513,9 +542,7 @@
         wait_bytes(again.at[pl.ds(0, group)], a_sem.at[1])
 
     wait_bytes(bbuf.at[pl.ds(0, nz - 1)], b_sem.at[1])
-    block = bbuf[0]
-    for i in range(1, nz):
-        block += bbuf[i]
+    block = tree_sum([bbuf[i] for i in range(nz)])
 
     @pl.when(at_lead)
     def _():
@@ -524,10 +551,7 @@
     @pl.when(jnp.logical_not(at_lead))
     def _():
         wait_bytes(zgain, c_sem.at[1])
-        gains = zgain[0]
-        for i in range(1, nz):
-            gains += zgain[i]
-        cbuf[...] = gains
+        cbuf[...] = tree_sum([zgain[i] for i in range(nz)])
 
     for h in range(2):
         taps = block[h : h + 1]
@@ -593,12 +617,12 @@
             pltpu.VMEM((nz, 1, LANES), f32),
             dma((6,)),
             dma((TILES + 1,)),
-            dma((2,)),
+            dma((3,)),
             dma((2,)),
             dma((4,)),
             dma((2,)),
             dma((2,)),
-            regular((6,)),
+            regular((7,)),
         ],
         compiler_params=pltpu.CompilerParams(collective_id=0, has_side_effects=True),
         name="segment_backward",

time: 42.5 us -> 41.8 us (0.984)
  Pallas kernels: 41.7 us -> 41 us
    pallas_call x1, Pallas kernels: 40.9 us -> 40.2 us  [per_device(): pl.pallas_call(functools.partial(body, sizes), out_shape=tuple((pltpu.VME...]
where the time goes in v5:
time: 41.8 us; the launch traced here: 41.7 us
  Pallas kernels  41 us (98%)
  between operations  0.64 us (2%)
    pallas_call x1, Pallas kernels, per_device(): pl.pallas_call(functools.partial(body, sizes), out_shape=tuple((pltpu.VME...  40.2 us

profile of v5, /device:TPU:1, one launch (start us, length us, event | category | flops | bytes accessed | tf_op | source)
XLA Modules:
  0.0 41.7 jit_solution(8791381360681782349)
XLA Ops:
  0.6 40.2 %segment_backward.1 = (bf16[512,128]{1,0:T(8,128)(2,1)S(1)}, bf16[512,128]{1,0:T(8,128)(2,1)S(1)}, bf16[512,128]{1,0:T(8,128)(2,1)S(1)}, f32[1,64]{1,0:T(1,128)S...) custom-call(bf16[512,128]{1,0:T(8,128)(2,1)} %q_hbm.1, bf16[512,128]{1,0:T(8,128)(2,1)} %k_hbm.1, bf16[512,128]{1,0:T(8,128)(2,1)} %v_hbm.1, ...), custom_call_target="tpu_custom_call" | custom-call | tf_op jit(solution)/shard_map/segment_backward/pallas_call | solution.py:594
  40.9 0.8 %flush.1 = (bf16[512,128]{1,0:T(8,128)(2,1)}, bf16[512,128]{1,0:T(8,128)(2,1)}, bf16[512,128]{1,0:T(8,128)(2,1)}, f32[1,64]{1,0:T(1,128)}, f32[1,64]{1,0:T(1,128)}, /*index=5*/f32[2,129]{1,0:T(2,128)}) custom-call(bf16[512,128]{1,0:T(8,128)(2,1)S(1)} %get-tuple-element.18.refs_0_, bf16[512,128]{1,0:T(8,128)(2,1)S(1)} %get-tuple-element.19.refs_1_, ...), custom_call_target="tpu_custom_call" | custom-call | tf_op jit(solution)/shard_map/flush/pallas_call | solution.py:630

commit v6 on v5

--- a/solution.py
+++ b/solution.py
@@ -224,7 +224,7 @@
         return pltpu.make_async_remote_copy(
             src_ref=src.at[tile],
             dst_ref=dst.at[tile],
-            send_sem=halo_send.at[2 if kind == 0 and tile < TILES - 1 else kind],
+            send_sem=halo_send.at[2 if kind == 0 and tile < TILES // 2 else kind],
             recv_sem=halo_recv.at[recv],
             device_id=at_sp(to),
             device_id_type=MESH,
@@ -306,7 +306,7 @@
 
     @pl.when(jnp.logical_not(at_lead))
     def _():
-        wait_bytes(kv_ref.at[TILES - 1], halo_send.at[0])
+        wait_bytes(kv_ref.at[pl.ds(TILES // 2, TILES // 2)], halo_send.at[0])
         tell(link_free, [{"c": lead}])
 
     @pl.when(at_lead)
@@ -348,7 +348,7 @@
             pl.semaphore_wait(level_2, len(two_away))
             tell(level_3, four_away)
             tell(x_ready, x_peers)
-        if ck == 0:
+        if ck == TILES - 2:
 
             @pl.when(at_lead)
             def _():
@@ -528,13 +528,13 @@
         ).astype(bf16)
 
     wait_bytes(qg_ref, halo_send.at[1])
-    wait_bytes(kv_ref.at[pl.ds(0, TILES - 1)], halo_send.at[2])
+    wait_bytes(kv_ref.at[pl.ds(0, TILES // 2)], halo_send.at[2])
     wait_bytes(send_stat, stat_sem.at[0])
     wait_bytes(abuf.at[pl.ds(0, ny - 1)], a_sem.at[0])
 
     @pl.when(at_lead)
     def _():
-        wait_bytes(kv_ref.at[TILES - 1], halo_send.at[0])
+        wait_bytes(kv_ref.at[pl.ds(TILES // 2, TILES // 2)], halo_send.at[0])
         wait_bytes(again.at[pl.ds(0, group - 1)], a_sem.at[1])
 
     @pl.when(jnp.logical_not(at_lead))

time: 41.8 us -> 41.8 us (level)
  no operation moved by 1% of the time
where the time goes in v6:
time: 41.8 us; the launch traced here: 41.6 us
  Pallas kernels  41 us (98%)
  between operations  0.64 us (2%)
    pallas_call x1, Pallas kernels, per_device(): pl.pallas_call(functools.partial(body, sizes), out_shape=tuple((pltpu.VME...  40.2 us

profile of v6, /device:TPU:1, one launch (start us, length us, event | category | flops | bytes accessed | tf_op | source)
XLA Modules:
  0.0 41.6 jit_solution(11656180190667206344)
XLA Ops:
  0.6 40.2 %segment_backward.1 = (bf16[512,128]{1,0:T(8,128)(2,1)S(1)}, bf16[512,128]{1,0:T(8,128)(2,1)S(1)}, bf16[512,128]{1,0:T(8,128)(2,1)S(1)}, f32[1,64]{1,0:T(1,128)S...) custom-call(bf16[512,128]{1,0:T(8,128)(2,1)} %q_hbm.1, bf16[512,128]{1,0:T(8,128)(2,1)} %k_hbm.1, bf16[512,128]{1,0:T(8,128)(2,1)} %v_hbm.1, ...), custom_call_target="tpu_custom_call" | custom-call | tf_op jit(solution)/shard_map/segment_backward/pallas_call | solution.py:594
  40.8 0.8 %flush.1 = (bf16[512,128]{1,0:T(8,128)(2,1)}, bf16[512,128]{1,0:T(8,128)(2,1)}, bf16[512,128]{1,0:T(8,128)(2,1)}, f32[1,64]{1,0:T(1,128)}, f32[1,64]{1,0:T(1,128)}, /*index=5*/f32[2,129]{1,0:T(2,128)}) custom-call(bf16[512,128]{1,0:T(8,128)(2,1)S(1)} %get-tuple-element.18.refs_0_, bf16[512,128]{1,0:T(8,128)(2,1)S(1)} %get-tuple-element.19.refs_1_, ...), custom_call_target="tpu_custom_call" | custom-call | tf_op jit(solution)/shard_map/flush/pallas_call | solution.py:630
